TPU v7x, 32 devices: a whole 2x2x4 slice. The times are simulated.
32 devices in a mesh: ep: 8 (over z, core), tp: 4 (over y, x).
Axes of the slice: x: 2, y: 2, z: 4, core: 2. Of those that a mesh axis runs over, the one named last changes fastest.
Arguments:
- tokens: bfloat16 [384, 2048], P('ep', 'tp'), may hold values from -64 to 64
- mix_gain: float32 [2048], replicated, may hold values from 0.1 to 1.9
- w_gate_z: bfloat16 [2048, 2048], P(None, 'tp'), may hold values from -0.125 to 0.125
- w_value_x: bfloat16 [2048, 2048], P(None, 'tp'), may hold values from -0.125 to 0.125
- w_key_b: bfloat16 [2048, 256], replicated, may hold values from -0.125 to 0.125
- w_query_c: bfloat16 [2048, 256], replicated, may hold values from -0.125 to 0.125
- w_step: bfloat16 [2048, 32], replicated, may hold values from -0.125 to 0.125
- step_bias: float32 [32], replicated, may hold values from -2 to 1
- decay_log: float32 [32], replicated, may hold values from -3 to 1.4
- skip_gain: float32 [32], replicated, may hold values from 0.1 to 1.9
- conv_x_weight: bfloat16 [4, 2048], P(None, 'tp'), may hold values from -3 to 3
- conv_b_weight: bfloat16 [4, 256], replicated, may hold values from -3 to 3
- conv_c_weight: bfloat16 [4, 256], replicated, may hold values from -3 to 3
- window_x: bfloat16 [384, 3, 2048], P('ep', None, 'tp'), may hold values from -6 to 6
- window_b: bfloat16 [384, 3, 256], P('ep'), may hold values from -6 to 6
- window_c: bfloat16 [384, 3, 256], P('ep'), may hold values from -6 to 6
- ssm_state: float32 [384, 32, 64, 128], P('ep', 'tp'), may hold values from -2 to 2
- head_gain: float32 [2048], P('tp'), may hold values from 0.1 to 1.9
- w_out: bfloat16 [2048, 2048], P('tp'), may hold values from -0.1875 to 0.1875
- ffn_gain: float32 [2048], replicated, may hold values from 0.1 to 1.9
- route_ids: int32 [384, 2], P('ep'), may hold values from 0 to 31, all different within a row; in each aligned block of 48 rows (0 to 47, 48 to 95, ...) at most 5 rows name the same one
- route_weights: float32 [384, 2], P('ep'), may hold values from 0.05 to 1
- expert_gate: bfloat16 [8, 2048, 4096], P('ep', None, 'tp'), may hold values from -0.125 to 0.125
- expert_up: bfloat16 [8, 2048, 4096], P('ep', None, 'tp'), may hold values from -0.125 to 0.125
- expert_down: bfloat16 [8, 4096, 2048], P('ep', 'tp'), may hold values from -0.25 to 0.25
Outputs:
- layer_out: bfloat16 [384, 2048], P('ep', 'tp')
Inputs may be any that keep to these rules, and one draw needn't show every extreme that they name: `route_ids`: each row names 2 different experts. Within the rows of one index of ep (aligned blocks of 48 rows) no expert is named by more than 5 rows, a bound that some block reaches.
All inputs are finite; a program needn't handle non-finite values.
Results may differ from a plain program's by a relative error of at most 0.009.
Values may be sent and summed in bfloat16 or wider, within the bound.
No kernel may reach another device: no remote copies, remote signals or barrier semaphores. Data moves between devices by JAX's collectives and lax.ppermute only.
A program may use at most 64 MiB of HBM per device.

v0:
```python
import jax
import jax.numpy as jnp
from jax import lax
from jax.sharding import PartitionSpec as P

HEADS = 32
HEAD_DIM = 64
STATE = 128
GROUPS = 2
EXP_IN = 4


norm_epsilon = 1e-06


def row_norm(arr_values, norm_gain):
    widened = arr_values.astype(jnp.float32)
    return (
        widened
        * lax.rsqrt(jnp.mean(widened * widened, axis=-1, keepdims=True) + norm_epsilon)
        * norm_gain
    )


def short_conv(window, fresh_row, weight):
    conv_taps = weight.astype(jnp.float32)
    summed = (
        jnp.sum(window.astype(jnp.float32) * conv_taps[:-1][None], axis=1)
        + fresh_row * conv_taps[-1]
    )
    return jax.nn.silu(summed)


def product(left, right):
    return jnp.dot(left, right, preferred_element_type=jnp.float32)


def local(
    tokens,
    mix_gain,
    w_gate_z,
    w_value_x,
    w_key_b,
    w_query_c,
    w_step,
    step_bias,
    decay_log,
    skip_gain,
    conv_x_weight,
    conv_b_weight,
    conv_c_weight,
    window_x,
    window_b,
    window_c,
    ssm_state,
    head_gain,
    w_out,
    ffn_gain,
    route_ids,
    route_weights,
    expert_gate,
    expert_up,
    expert_down,
):
    tp_index = lax.axis_index("tp")
    tp_count = lax.axis_size("tp")
    ep_count = lax.axis_size("ep")
    seq_count = tokens.shape[0]
    gathered = lax.all_gather(tokens, "tp", axis=1, tiled=True)
    normed = row_norm(gathered, mix_gain).astype(jnp.bfloat16)
    local_width = w_gate_z.shape[1]
    head_count = local_width // HEAD_DIM
    first_head = tp_index * head_count
    group_start = first_head // (HEADS // GROUPS) * STATE
    gate_z = product(normed, w_gate_z)
    values = short_conv(window_x, product(normed, w_value_x), conv_x_weight)
    key_b = short_conv(
        lax.dynamic_slice_in_dim(window_b, group_start, STATE, 2),
        product(normed, lax.dynamic_slice_in_dim(w_key_b, group_start, STATE, 1)),
        lax.dynamic_slice_in_dim(conv_b_weight, group_start, STATE, 1),
    )
    query_c = short_conv(
        lax.dynamic_slice_in_dim(window_c, group_start, STATE, 2),
        product(normed, lax.dynamic_slice_in_dim(w_query_c, group_start, STATE, 1)),
        lax.dynamic_slice_in_dim(conv_c_weight, group_start, STATE, 1),
    )
    step_all = product(normed, w_step) + step_bias
    step_size = jax.nn.softplus(lax.dynamic_slice_in_dim(step_all, first_head, head_count, 1))
    rate_heads = jnp.exp(lax.dynamic_slice_in_dim(decay_log, first_head, head_count, 0))
    skip_heads = lax.dynamic_slice_in_dim(skip_gain, first_head, head_count, 0)
    decay_heads = jnp.exp(-step_size * rate_heads)
    value_heads = values.reshape(seq_count, head_count, HEAD_DIM)
    new_state = (
        decay_heads[:, :, None, None] * ssm_state
        + (step_size[:, :, None] * value_heads)[..., None] * key_b[:, None, None, :]
    )
    read_out = jnp.einsum("shpn,sn->shp", new_state, query_c, precision=lax.Precision.HIGHEST)
    read_out = read_out + skip_heads[None, :, None] * value_heads
    gated = read_out * jax.nn.silu(gate_z.reshape(seq_count, head_count, HEAD_DIM))
    gated = gated * lax.rsqrt(jnp.mean(gated * gated, axis=-1, keepdims=True) + norm_epsilon)
    mixed_heads = (
        (gated * head_gain.reshape(head_count, HEAD_DIM))
        .reshape(seq_count, local_width)
        .astype(jnp.bfloat16)
    )
    partial_value = product(mixed_heads, w_out)
    share_mix = lax.psum_scatter(partial_value, "tp", scatter_dimension=1, tiled=True)
    residual_own = (tokens.astype(jnp.float32) + share_mix).astype(jnp.bfloat16)
    residual_full = lax.all_gather(residual_own, "tp", axis=1, tiled=True)
    ffn_in = row_norm(residual_full, ffn_gain).astype(jnp.bfloat16)
    top_count = route_ids.shape[1]
    expert_count = EXP_IN * ep_count
    capacity = max(2, (3 * seq_count * top_count + 2 * expert_count - 1) // (2 * expert_count))
    sub_index = tp_index // (tp_count // EXP_IN)
    target_set = route_ids // EXP_IN
    hit_mask = route_ids % EXP_IN == sub_index
    set_grid = jnp.arange(ep_count, dtype=jnp.int32)
    set_onehot = (hit_mask[:, :, None] & (target_set[:, :, None] == set_grid)).astype(jnp.int32)
    set_onehot = set_onehot.reshape(seq_count * top_count, ep_count)
    earlier = jnp.cumsum(set_onehot, axis=0) - set_onehot
    slot_rank = jnp.sum(earlier * set_onehot, axis=1).reshape(seq_count, top_count)
    slot_index = jnp.where(hit_mask, target_set * capacity + slot_rank, -1)
    slot_grid = jnp.arange(ep_count * capacity, dtype=jnp.int32)
    slot_match = slot_index[:, :, None] == slot_grid
    placed = jnp.any(slot_match, axis=1).astype(jnp.bfloat16)
    outgoing = jnp.einsum("sj,sd->jd", placed, ffn_in, preferred_element_type=jnp.float32)
    outgoing = outgoing.astype(jnp.bfloat16).reshape(ep_count, capacity, ffn_in.shape[1])
    route_share = route_weights / jnp.sum(route_weights, axis=1, keepdims=True)
    combine_weight = jnp.sum(jnp.where(slot_match, route_share[:, :, None], 0.0), axis=1)
    arrived = lax.all_to_all(outgoing, "ep", split_axis=0, concat_axis=0, tiled=True)
    source_count, slot_count, row_width = arrived.shape
    flat_rows = arrived.reshape(source_count * slot_count, row_width)
    gate_part = product(flat_rows, expert_gate[0])
    up_part = product(flat_rows, expert_up[0])
    hidden = (jax.nn.silu(gate_part) * up_part).astype(jnp.bfloat16)
    expert_out = product(hidden, expert_down[0]).reshape(source_count, slot_count, row_width)
    returned = lax.all_to_all(
        expert_out.astype(jnp.bfloat16), "ep", split_axis=0, concat_axis=0, tiled=True
    ).astype(expert_out.dtype)
    moe_part = jnp.dot(
        combine_weight,
        returned.reshape(ep_count * capacity, -1),
        precision=lax.Precision.HIGHEST,
        preferred_element_type=jnp.float32,
    )
    moe_share = lax.psum_scatter(
        moe_part.astype(jnp.bfloat16), "tp", scatter_dimension=1, tiled=True
    ).astype(jnp.float32)
    return (residual_own.astype(jnp.float32) + moe_share).astype(jnp.bfloat16)


def solution(mesh):
    in_specs = (
        P("ep", "tp"),
        P(),
        P(None, "tp"),
        P(None, "tp"),
        P(),
        P(),
        P(),
        P(),
        P(),
        P(),
        P(None, "tp"),
        P(),
        P(),
        P("ep", None, "tp"),
        P("ep", None, None),
        P("ep", None, None),
        P("ep", "tp", None, None),
        P("tp"),
        P("tp", None),
        P(),
        P("ep", None),
        P("ep", None),
        P("ep", None, "tp"),
        P("ep", None, "tp"),
        P("ep", "tp", None),
    )
    out_specs = P("ep", "tp")
    return jax.shard_map(local, mesh=mesh, in_specs=in_specs, out_specs=out_specs, check_vma=False)
```

profile of v0, /device:TPU:0, one launch (start us, length us, event | category | flops | bytes accessed | tf_op | source)
XLA Modules:
  0.0 169.4 jit_solution(5472873604059816958)
XLA Ops:
  6.5 0.0 reduce-scatter.3.cloned.1.call-start
  6.6 0.8 slice.24
  7.4 0.7 slice.25
  8.1 0.7 fusion.50
  8.8 0.7 fusion.49
  9.5 10.4 %all_gather.6 = bf16[48,2048]{1,0:T(8,128)(2,1)S(1)} all-gather(bf16[48,512]{1,0:T(8,128)(2,1)} %param.25), channel_id=1, replica_groups=mesh['ep'=8,'tp'=4] {'tp'}, dimensions={1}, use_global_device_ids=true | all-gather | bytes 245760 | tf_op jit(solution)/shard_map/all_gather | solution.py:69
  19.9 0.1 fusion.27
  20.1 0.7 dynamic-slice
  20.8 0.7 dynamic-slice_exponential_fusion
  21.6 1.2 fusion.56
  22.7 0.1 multiply_exponential_fusion
  22.8 0.1 copy.87
  22.9 1.0 multiply_reduce_fusion
  23.9 2.1 %divide_multiply_fusion = f32[48,512]{1,0:T(8,128)S(1)} fusion(f32[48,512]{1,0:T(8,128)S(1)} %multiply_reduce_fusion, bf16[2048,512]{1,0:T(8,128)(2,1)} %param.28, f32[512]{0:T(512)S(1)} %bitcast.43, bf16[48,2048]{1,0:T(8,128)(2,1)S(1)} %all_gather.6, f32[2048]{0:T(1024)} %param.26, f32[48]{0:T(128)S(1)} %add_rsqrt_fusion.2), kind=kOutput, calls=%fused_computation.44 | convolution fusion | flops 101203968 | bytes 2500800 | tf_op jit(solution)/shard_map/dot_general | solution.py:35
  26.0 0.1 reshape.73
  26.1 0.1 copy.86
  26.2 0.7 dynamic_slice.35
  26.9 2.1 %fusion.51 = f32[48,512]{1,0:T(8,128)S(1)} fusion(bf16[2048,512]{1,0:T(8,128)(2,1)} %param.27, bf16[48,2048]{1,0:T(8,128)(2,1)S(1)} %all_gather.6, f32[2048]{0:T(1024)} %param.26, f32[48]{0:T(128)S(1)} %add_rsqrt_fusion.2), kind=kOutput, calls=%fused_computation.85 | convolution fusion | flops 101056512 | bytes 2400448 | tf_op jit(solution)/shard_map/dot_general | solution.py:35
  29.1 0.1 reshape.74
  29.2 0.1 broadcast_multiply_fusion
  29.4 1.3 divide_multiply_fusion.2
  30.7 1.3 divide_multiply_fusion.1
  32.0 31.9 %fusion = f32[48,1,8,64]{3,1,2,0:T(1,128)S(1)} fusion(f32[48,128,1,1]{1,2,3,0:T(1,128)S(1)} %bitcast.40, f32[48,8,64,128]{3,2,1,0:T(8,128)} %param.41, f32[48,128]{1,0:T(8,128)S(1)} %divide_multiply_fusion.2, f32[48,8,64]{2,1,0:T(8,128)S(1)} %broadcast_multiply_fusion, f32[48,8]{1,0:T(8,128)S(1)} %copy.86), kind=kOutput, calls=%fused_computation | convolution fusion | flops 47185920 | bytes 12830208 | tf_op jit(solution)/shard_map/shpn,sn->shp/dot_general | solution.py:97
  63.9 0.0 copy-start.2
  63.9 0.0 copy-start.6
  64.0 0.2 multiply_reduce_fusion.1
  64.2 0.1 copy.88
  64.2 0.1 copy.89
  64.3 0.1 mul.243
  64.4 0.1 multiply_convert_fusion
  64.5 0.1 convert_element_type.79
  64.7 1.2 fusion.58
  65.9 0.0 reduce-scatter.3.cloned.1.call-update
  65.9 0.1 copy.91
  66.0 0.1 copy.94
  66.2 0.1 and.32
  66.3 0.1 eq.39
  66.5 0.1 fusion.38
  66.6 0.1 reduce_window_sum.11
  66.7 0.2 select_reduce_fusion
  66.9 0.1 reshape.75
  67.0 0.1 copy.97
  67.1 24.0 %reduce-scatter.3.cloned.1.call-done = f32[48,512]{1,0:T(8,128)} async-done(((f32[48,2048]{1,0:T(8,128)}), f32[48,512]{1,0:T(8,128)}) %reduce-scatter.3.cloned.1.call-update) | async-done | bytes 98320 | tf_op jit(solution)/shard_map/reduce_scatter | solution.py:107
  91.1 0.9 add_convert_fusion.1
  92.0 8.9 %all_gather.7 = bf16[48,2048]{1,0:T(8,128)(2,1)S(1)} all-gather(bf16[48,512]{1,0:T(8,128)(2,1)S(1)} %add_convert_fusion.1), channel_id=1, replica_groups=mesh['ep'=8,'tp'=4] {'tp'}, dimensions={1}, use_global_device_ids=true | all-gather | bytes 245760 | tf_op jit(solution)/shard_map/all_gather | solution.py:109
  100.9 0.1 fusion.30
  101.1 0.3 convolution_convert_fusion.1
  101.4 0.8 reshape.76
  102.1 4.6 %all-to-all-start = ((bf16[8,5,2048]{2,1,0:T(8,128)(2,1)}), bf16[8,5,2048]{2,1,0:T(8,128)(2,1)S(1)}, u32[]{:S(2)}, u32[]{:S(2)}) async-start(bf16[8,5,2048]{2,1,0:T(8,128)(2,1)} %reshape.76), calls=%async_computation.1 | async-start | bytes 524288 | tf_op jit(solution)/shard_map/all_to_all | solution.py:130
  106.7 9.7 %all-to-all-done = bf16[8,5,2048]{2,1,0:T(8,128)(2,1)S(1)} async-done(((bf16[8,5,2048]{2,1,0:T(8,128)(2,1)}), bf16[8,5,2048]{2,1,0:T(8,128)(2,1)S(1)}, u32[]{:S(2)}, u32[]{:S(2)}) %all-to-all-start) | async-done | bytes 163872 | tf_op jit(solution)/shard_map/all_to_all | solution.py:130
  116.4 0.1 reshape.77
  116.5 3.2 %fusion.11 = f32[40,1024]{1,0:T(8,128)S(1)} fusion(bf16[40,2048]{1,0:T(8,128)(2,1)S(1)} %reshape.77, bf16[1,2048,1024]{2,1,0:T(8,128)(2,1)} %param.47), kind=kOutput, calls=%fused_computation.11 | convolution fusion | flops 167772160 | bytes 4521984 | tf_op jit(solution)/shard_map/dot_general | solution.py:35
  119.7 0.3 copy-done.1
  120.0 0.8 fusion.19
  120.9 3.0 %fusion.13 = bf16[8,5,2048]{2,0,1:T(8,128)(2,1)S(1)} fusion(bf16[1,1024,2048]{2,1,0:T(8,128)(2,1)} %param.49, bf16[8,5,1024]{2,1,0:T(8,128)(2,1)S(1)} %dot_general.48), kind=kOutput, calls=%fused_computation.14 | convolution fusion | flops 167854080 | bytes 4440064 | tf_op jit(solution)/shard_map/dot_general | solution.py:35
  123.8 0.8 copy.99
  124.6 3.4 %all-to-all-start.1 = ((bf16[8,5,2048]{2,1,0:T(8,128)(2,1)}), bf16[8,5,2048]{2,1,0:T(8,128)(2,1)S(1)}, u32[]{:S(2)}, u32[]{:S(2)}) async-start(bf16[8,5,2048]{2,1,0:T(8,128)(2,1)} %copy.99), calls=%async_computation.2 | async-start | bytes 524288 | tf_op jit(solution)/shard_map/all_to_all | solution.py:137
  128.0 0.0 reduce-scatter.5.cloned.1.call-start
  128.1 9.6 %all-to-all-done.1 = bf16[8,5,2048]{2,1,0:T(8,128)(2,1)S(1)} async-done(((bf16[8,5,2048]{2,1,0:T(8,128)(2,1)}), bf16[8,5,2048]{2,1,0:T(8,128)(2,1)S(1)}, u32[]{:S(2)}, u32[]{:S(2)}) %all-to-all-start.1) | async-done | bytes 163872 | tf_op jit(solution)/shard_map/all_to_all | solution.py:137
  137.7 0.1 reshape.78
  137.8 1.0 convolution_convert_fusion
  138.8 0.0 reduce-scatter.5.cloned.1.call-update
  138.8 22.3 %reduce-scatter.5.cloned.1.call-done = bf16[48,512]{1,0:T(8,128)(2,1)} async-done(((bf16[48,2048]{1,0:T(8,128)(2,1)}), bf16[48,512]{1,0:T(8,128)(2,1)}) %reduce-scatter.5.cloned.1.call-update) | async-done | bytes 49168 | tf_op jit(solution)/shard_map/reduce_scatter | solution.py:146
  161.1 1.4 add_convert_fusion
  (32 shorter events, 0.3 us)
Async XLA Ops:
  6.5 58.1 %copy-start = (bf16[512,2048]{1,0:T(8,128)(2,1)S(1)}, bf16[512,2048]{1,0:T(8,128)(2,1)}, u32[]{:S(2)}) copy-start(bf16[512,2048]{1,0:T(8,128)(2,1)} %param.43) | copy-start | bytes 6291460
  6.5 22.8 %copy-start.3 = (f32[2048]{0:T(1024)S(1)}, f32[2048]{0:T(1024)}, u32[]{:S(2)}) copy-start(f32[2048]{0:T(1024)} %param.26) | copy-start | bytes 24580
  6.5 22.8 %copy-start.5 = (bf16[48,3,256]{2,0,1:T(8,128)(2,1)S(1)}, bf16[48,3,256]{2,0,1:T(8,128)(2,1)}, u32[]{:S(2)}) copy-start(bf16[48,3,256]{2,0,1:T(8,128)(2,1)} %param.39) | copy-start | bytes 221188
  6.5 22.8 %copy-start.4 = (bf16[48,3,256]{2,0,1:T(8,128)(2,1)S(1)}, bf16[48,3,256]{2,0,1:T(8,128)(2,1)}, u32[]{:S(2)}) copy-start(bf16[48,3,256]{2,0,1:T(8,128)(2,1)} %param.40) | copy-start | bytes 221188
  6.5 84.5 %reduce-scatter.3.cloned.1.call-start = ((), (), s32[]{:S(2)}) async-start(), calls=%async_computation.4 | async-start | bytes 491520 | tf_op jit(solution)/shard_map/reduce_scatter | solution.py:107
  32.0 32.3 %copy-start.8 = (f32[512]{0:T(512)S(1)}, f32[512]{0:T(512)}, u32[]{:S(2)}) copy-start(f32[512]{0:T(512)} %param.42) | copy-start | bytes 6148
  63.9 2.0 %copy-start.9 = (s32[48,2]{0,1:T(2,128)S(1)}, s32[48,2]{0,1:T(2,128)}, u32[]{:S(2)}) copy-start(s32[48,2]{0,1:T(2,128)} %param.45) | copy-start | bytes 1156
  63.9 27.2 %copy-start.2 = (bf16[48,512]{1,0:T(8,128)(2,1)S(1)}, bf16[48,512]{1,0:T(8,128)(2,1)}, u32[]{:S(2)}) copy-start(bf16[48,512]{1,0:T(8,128)(2,1)} %param.25) | copy-start | bytes 147460
  63.9 37.2 %copy-start.6 = (f32[2048]{0:T(1024)S(1)}, f32[2048]{0:T(1024)}, u32[]{:S(2)}) copy-start(f32[2048]{0:T(1024)} %param.44) | copy-start | bytes 24580
  64.0 42.8 %copy-start.7 = (f32[48,2]{0,1:T(2,128)S(1)}, f32[48,2]{0,1:T(2,128)}, u32[]{:S(2)}) copy-start(f32[48,2]{0,1:T(2,128)} %param.46) | copy-start | bytes 1156
  102.1 14.3 %all-to-all-start = ((bf16[8,5,2048]{2,1,0:T(8,128)(2,1)}), bf16[8,5,2048]{2,1,0:T(8,128)(2,1)S(1)}, u32[]{:S(2)}, u32[]{:S(2)}) async-start(bf16[8,5,2048]{2,1,0:T(8,128)(2,1)} %reshape.76), calls=%async_computation.1 | async-start | bytes 524288 | tf_op jit(solution)/shard_map/all_to_all | solution.py:130
  116.5 3.5 %copy-start.1 = (bf16[1,2048,1024]{2,1,0:T(8,128)(2,1)S(1)}, bf16[1,2048,1024]{2,1,0:T(8,128)(2,1)}, u32[]{:S(2)}) copy-start(bf16[1,2048,1024]{2,1,0:T(8,128)(2,1)} %param.48) | copy-start | bytes 12582916
  124.6 13.1 %all-to-all-start.1 = ((bf16[8,5,2048]{2,1,0:T(8,128)(2,1)}), bf16[8,5,2048]{2,1,0:T(8,128)(2,1)S(1)}, u32[]{:S(2)}, u32[]{:S(2)}) async-start(bf16[8,5,2048]{2,1,0:T(8,128)(2,1)} %copy.99), calls=%async_computation.2 | async-start | bytes 524288 | tf_op jit(solution)/shard_map/all_to_all | solution.py:137
  128.0 33.1 %reduce-scatter.5.cloned.1.call-start = ((), (), s32[]{:S(2)}) async-start(), calls=%async_computation.5 | async-start | bytes 245760 | tf_op jit(solution)/shard_map/reduce_scatter | solution.py:146
Sparse Core Ops, SparseCore 0:
  66.1 24.9 reduce-scatter.2
  138.9 22.1 reduce-scatter.4
where the time goes:
time: 170 us; the launch traced here: 169 us
  waiting for transfers between devices  65.6 us (39%)
  matrix products  49.5 us (29%)
  blocking collectives  19.4 us (11%)
  between operations  13.7 us (8%)
  starting transfers between devices  8.08 us (5%)
  local copies, waits for them, and re-layouts  7.17 us (4%)
  other arithmetic  6.07 us (4%)
    dot_general x1, matrix products, local(): jnp.einsum('shpn,sn->shp', new_state, query_c, precision=lax.Precision.HI...  31.9 us
    reduce_scatter x1, waiting for transfers between devices, local(): lax.psum_scatter(partial_value, 'tp', scatter_dimension=1, tiled=True)  24 us
    reduce_scatter x1, waiting for transfers between devices, local(): lax.psum_scatter(moe_part.astype(jnp.bfloat16), 'tp', scatter_dimension=1...  22.3 us
    dot_general x9, matrix products, product(): return jnp.dot(left, right, preferred_element_type=jnp.float32)  16.3 us
    all_gather x1, blocking collectives, local(): gathered = lax.all_gather(tokens, 'tp', axis=1, tiled=True)  10.4 us
    all_to_all x1, waiting for transfers between devices, local(): lax.all_to_all(outgoing, 'ep', split_axis=0, concat_axis=0, tiled=True)  9.68 us
    all_to_all x1, waiting for transfers between devices, local(): lax.all_to_all(expert_out.astype(jnp.bfloat16), 'ep', split_axis=0, conca...  9.55 us
    all_gather x1, blocking collectives, local(): residual_full = lax.all_gather(residual_own, 'tp', axis=1, tiled=True)  8.94 us
  transfers between devices with their start and end apart: 4, of which 4 were waited for; matrix products, arithmetic and copies ran while one was open for 1% of the time, Pallas kernels for 0%

commit v1 on v0

--- a/solution.py
+++ b/solution.py
@@ -1,6 +1,8 @@
 import jax
 import jax.numpy as jnp
 from jax import lax
+from jax.experimental import pallas as pl
+from jax.experimental.pallas import tpu as pltpu
 from jax.sharding import PartitionSpec as P
 
 HEADS = 32
@@ -35,7 +37,7 @@
     return jnp.dot(left, right, preferred_element_type=jnp.float32)
 
 
-def local(
+def local_generic(
     tokens,
     mix_gain,
     w_gate_z,
@@ -149,6 +151,373 @@
     return (residual_own.astype(jnp.float32) + moe_share).astype(jnp.bfloat16)
 
 
+ROW_TILE = 8
+LANES = 128
+
+
+def dot_bf16(left, right):
+    return lax.dot_general(left, right, (((1,), (0,)), ((), ())), preferred_element_type=jnp.float32)
+
+
+def dot_nt(left, right, precision=None):
+    return lax.dot_general(
+        left, right, (((1,), (1,)), ((), ())), precision=precision, preferred_element_type=jnp.float32
+    )
+
+
+def dot_exact(left, right):
+    return lax.dot_general(
+        left,
+        right,
+        (((1,), (0,)), ((), ())),
+        precision=lax.Precision.HIGHEST,
+        preferred_element_type=jnp.float32,
+    )
+
+
+def silu(value):
+    return value / (1.0 + jnp.exp(-value))
+
+
+def conv_rows(window_ref, columns, fresh, taps_ref):
+    taps = taps_ref[:, columns].astype(jnp.float32)
+    count = window_ref.shape[0]
+    summed = fresh * taps[count : count + 1]
+    for tap in range(count):
+        summed = summed + window_ref[tap, :, columns].astype(jnp.float32) * taps[tap : tap + 1]
+    return silu(summed)
+
+
+def mixer_body(
+    row_ref,
+    gain_ref,
+    step_w_ref,
+    bias_ref,
+    rate_ref,
+    skip_ref,
+    tap_x_ref,
+    tap_b_ref,
+    tap_c_ref,
+    win_x_ref,
+    win_b_ref,
+    win_c_ref,
+    head_gain_ref,
+    gate_hbm,
+    value_hbm,
+    key_hbm,
+    query_hbm,
+    state_hbm,
+    out_w_hbm,
+    part_ref,
+    gate_w,
+    value_w,
+    key_w,
+    query_w,
+    state,
+    out_w,
+    y_ref,
+    w_sems,
+    s_sems,
+):
+    tp_index = lax.axis_index("tp")
+    seqs, width = y_ref.shape
+    head_count = width // HEAD_DIM
+    first_head = tp_index * head_count
+    group = first_head // (HEADS // GROUPS)
+    columns = pl.ds(pl.multiple_of(group * STATE, STATE), STATE)
+    copies = [
+        pltpu.make_async_copy(key_hbm.at[:, columns], key_w, w_sems.at[0]),
+        pltpu.make_async_copy(query_hbm.at[:, columns], query_w, w_sems.at[1]),
+        pltpu.make_async_copy(value_hbm, value_w, w_sems.at[2]),
+        pltpu.make_async_copy(gate_hbm, gate_w, w_sems.at[3]),
+        pltpu.make_async_copy(out_w_hbm, out_w, w_sems.at[4]),
+    ]
+    blocks = seqs // ROW_TILE
+    state_copies = [
+        pltpu.make_async_copy(
+            state_hbm.at[pl.ds(b * ROW_TILE, ROW_TILE)], state.at[pl.ds(b * ROW_TILE, ROW_TILE)], s_sems.at[b]
+        )
+        for b in range(blocks)
+    ]
+    for copy in copies[:2] + state_copies + copies[2:]:
+        copy.start()
+    rows = row_ref[...].astype(jnp.float32)
+    scale = lax.rsqrt(jnp.mean(rows * rows, axis=-1, keepdims=True) + norm_epsilon)
+    normed = (rows * scale * gain_ref[...]).astype(jnp.bfloat16)
+    step_size = jax.nn.softplus(dot_nt(normed, step_w_ref[...]) + bias_ref[...])
+    decay = jnp.exp(-step_size * jnp.exp(rate_ref[...]))
+    copies[0].wait()
+    keys = conv_rows(win_b_ref, columns, dot_bf16(normed, key_w[...]), tap_b_ref)
+    copies[1].wait()
+    queries = conv_rows(win_c_ref, columns, dot_bf16(normed, query_w[...]), tap_c_ref)
+    overlap = jnp.sum(keys * queries, axis=-1, keepdims=True)
+    query_hi = queries.astype(jnp.bfloat16)
+    query_lo = (queries - query_hi.astype(jnp.float32)).astype(jnp.bfloat16)
+    row_of = lax.broadcasted_iota(jnp.int32, (ROW_TILE, width), 0)
+    for b in range(blocks):
+        state_copies[b].wait()
+        lines = slice(b * ROW_TILE, (b + 1) * ROW_TILE)
+        both = jnp.concatenate([query_hi[lines], query_lo[lines]], axis=0)
+        total = jnp.zeros((ROW_TILE, width), jnp.float32)
+        for i in range(ROW_TILE):
+            found = dot_nt(both, state[b * ROW_TILE + i].astype(jnp.bfloat16))
+            total = jnp.where(row_of == i, found[:ROW_TILE] + found[ROW_TILE:], total)
+        y_ref[lines] = total
+    spread = (
+        lax.broadcasted_iota(jnp.int32, (HEADS, width), 0)
+        == first_head + lax.broadcasted_iota(jnp.int32, (HEADS, width), 1) // HEAD_DIM
+    ).astype(jnp.float32)
+    copies[2].wait()
+    values = conv_rows(win_x_ref, slice(None), dot_bf16(normed, value_w[...]), tap_x_ref)
+    copies[3].wait()
+    gate_z = dot_bf16(normed, gate_w[...])
+    read_out = (
+        dot_exact(decay, spread) * y_ref[...]
+        + (dot_exact(step_size, spread) * overlap + dot_exact(skip_ref[...], spread)) * values
+    )
+    gated = read_out * silu(gate_z)
+    mean_sq = dot_nt(gated * gated, spread, lax.Precision.HIGHEST) * (1.0 / HEAD_DIM)
+    scale_heads = dot_exact(lax.rsqrt(mean_sq + norm_epsilon), spread)
+    mixed = (gated * scale_heads * head_gain_ref[...]).astype(jnp.bfloat16)
+    copies[4].wait()
+    part_width = part_ref.shape[2]
+    for j in range(part_ref.shape[0]):
+        part_ref[j] = dot_bf16(mixed, out_w[:, j * part_width : (j + 1) * part_width]).astype(jnp.bfloat16)
+
+
+def slots_of(ids_ref, experts):
+    seqs = ids_ref.shape[1]
+    shape = (experts * ROW_TILE, seqs)
+    line = lax.broadcasted_iota(jnp.int32, shape, 0)
+    expert = line // ROW_TILE
+    first = ids_ref[0:1, :] == expert
+    second = ids_ref[1:2, :] == expert
+    hit = jnp.logical_or(first, second)
+    before = (
+        lax.broadcasted_iota(jnp.int32, (seqs, seqs), 0) < lax.broadcasted_iota(jnp.int32, (seqs, seqs), 1)
+    ).astype(jnp.bfloat16)
+    rank = dot_bf16(hit.astype(jnp.bfloat16), before)
+    place = (line % ROW_TILE).astype(jnp.float32)
+    return jnp.logical_and(hit, rank == place), first
+
+
+def pack_body(part_ref, own_ref, ids_ref, residual_ref, outgoing_ref):
+    total = own_ref[...].astype(jnp.float32)
+    share = part_ref[0].astype(jnp.float32)
+    for j in range(1, part_ref.shape[0]):
+        share = share + part_ref[j].astype(jnp.float32)
+    residual = (total + share).astype(jnp.bfloat16)
+    residual_ref[...] = residual
+    chosen, unused = slots_of(ids_ref, outgoing_ref.shape[0] // ROW_TILE)
+    outgoing_ref[...] = dot_bf16(chosen.astype(jnp.bfloat16), residual).astype(jnp.bfloat16)
+
+
+def expert_body(
+    arrived_ref, gain_ref, gate_hbm, up_hbm, down_hbm, result_ref, gate_w, up_w, down_w, x_ref, sems
+):
+    pieces = sems.shape[1]
+    copies = []
+    for piece in range(pieces):
+        for which, (source, target) in enumerate(((gate_hbm, gate_w), (up_hbm, up_w))):
+            lines = source.shape[0] // pieces
+            span = pl.ds(piece * lines, lines)
+            copies.append(pltpu.make_async_copy(source.at[span], target.at[span], sems.at[which, piece]))
+    lines_down = down_hbm.shape[0] // pieces
+    down_copies = [
+        pltpu.make_async_copy(
+            down_hbm.at[pl.ds(piece * lines_down, lines_down)],
+            down_w.at[pl.ds(piece * lines_down, lines_down)],
+            sems.at[2, piece],
+        )
+        for piece in range(pieces)
+    ]
+    for copy in copies + down_copies:
+        copy.start()
+    tp_count = lax.axis_size("tp")
+    ep_count = lax.axis_size("ep")
+    own_width = arrived_ref.shape[1]
+    for source in range(ep_count):
+        for part in range(tp_count):
+            x_ref[source * ROW_TILE : (source + 1) * ROW_TILE, part * own_width : (part + 1) * own_width] = (
+                arrived_ref[pl.ds((source * tp_count + part) * ROW_TILE, ROW_TILE), :].astype(jnp.float32)
+            )
+    rows = x_ref[...]
+    scale = lax.rsqrt(jnp.mean(rows * rows, axis=-1, keepdims=True) + norm_epsilon)
+    ffn_in = (rows * scale * gain_ref[...]).astype(jnp.bfloat16)
+    gate_part = 0.0
+    up_part = 0.0
+    lines = gate_hbm.shape[0] // pieces
+    for piece in range(pieces):
+        span = slice(piece * lines, (piece + 1) * lines)
+        copies[2 * piece].wait()
+        gate_part = gate_part + dot_bf16(ffn_in[:, span], gate_w[span])
+        copies[2 * piece + 1].wait()
+        up_part = up_part + dot_bf16(ffn_in[:, span], up_w[span])
+    hidden = (silu(gate_part) * up_part).astype(jnp.bfloat16)
+    result = 0.0
+    for piece in range(pieces):
+        span = slice(piece * lines_down, (piece + 1) * lines_down)
+        down_copies[piece].wait()
+        result = result + dot_bf16(hidden[:, span], down_w[span])
+    for source in range(ep_count):
+        for part in range(tp_count):
+            result_ref[pl.ds((source * tp_count + part) * ROW_TILE, ROW_TILE), :] = result[
+                source * ROW_TILE : (source + 1) * ROW_TILE, part * own_width : (part + 1) * own_width
+            ].astype(jnp.bfloat16)
+
+
+def combine_body(returned_ref, residual_ref, ids_ref, weight_ref, out_ref):
+    chosen, first = slots_of(ids_ref, returned_ref.shape[0] // ROW_TILE)
+    weights = weight_ref[...]
+    share = weights / jnp.sum(weights, axis=0, keepdims=True)
+    picked = jnp.where(chosen, jnp.where(first, share[0:1, :], share[1:2, :]), 0.0)
+    high = picked.astype(jnp.bfloat16)
+    low = (picked - high.astype(jnp.float32)).astype(jnp.bfloat16)
+    returned = returned_ref[...]
+    dims = (((0,), (0,)), ((), ()))
+    moe_sum = lax.dot_general(high, returned, dims, preferred_element_type=jnp.float32)
+    moe_sum = moe_sum + lax.dot_general(low, returned, dims, preferred_element_type=jnp.float32)
+    out_ref[...] = (residual_ref[...].astype(jnp.float32) + moe_sum).astype(jnp.bfloat16)
+
+
+IN_VMEM = pl.BlockSpec(memory_space=pltpu.VMEM)
+IN_HBM = pl.BlockSpec(memory_space=pltpu.HBM)
+
+
+def local_fast(
+    tokens,
+    mix_gain,
+    w_gate_z,
+    w_value_x,
+    w_key_b,
+    w_query_c,
+    w_step,
+    step_bias,
+    decay_log,
+    skip_gain,
+    conv_x_weight,
+    conv_b_weight,
+    conv_c_weight,
+    window_x,
+    window_b,
+    window_c,
+    ssm_state,
+    head_gain,
+    w_out,
+    ffn_gain,
+    route_ids,
+    route_weights,
+    expert_gate,
+    expert_up,
+    expert_down,
+):
+    tp_count = lax.axis_size("tp")
+    ep_count = lax.axis_size("ep")
+    seqs, own_width = tokens.shape
+    model_width = w_gate_z.shape[0]
+    width = w_gate_z.shape[1]
+    devices = ep_count * tp_count
+    bf16 = jnp.bfloat16
+    gathered = lax.all_gather(tokens, "tp", axis=1, tiled=True)
+    parts = pl.pallas_call(
+        mixer_body,
+        out_shape=jax.ShapeDtypeStruct((tp_count, seqs, own_width), bf16),
+        in_specs=[IN_VMEM] * 13 + [IN_HBM] * 6,
+        out_specs=IN_VMEM,
+        scratch_shapes=[
+            pltpu.VMEM((model_width, width), bf16),
+            pltpu.VMEM((model_width, width), bf16),
+            pltpu.VMEM((model_width, STATE), bf16),
+            pltpu.VMEM((model_width, STATE), bf16),
+            pltpu.VMEM((seqs, width, STATE), jnp.float32),
+            pltpu.VMEM((width, model_width), bf16),
+            pltpu.VMEM((seqs, width), jnp.float32),
+            pltpu.SemaphoreType.DMA((5,)),
+            pltpu.SemaphoreType.DMA((seqs // ROW_TILE,)),
+        ],
+        name="mixer",
+    )(
+        gathered,
+        mix_gain[None],
+        w_step.T,
+        step_bias[None],
+        decay_log[None],
+        skip_gain[None],
+        conv_x_weight,
+        conv_b_weight,
+        conv_c_weight,
+        jnp.swapaxes(window_x, 0, 1),
+        jnp.swapaxes(window_b, 0, 1),
+        jnp.swapaxes(window_c, 0, 1),
+        head_gain[None],
+        w_gate_z,
+        w_value_x,
+        w_key_b,
+        w_query_c,
+        ssm_state.reshape(seqs, width, STATE),
+        w_out,
+    )
+    shares = lax.all_to_all(parts, "tp", split_axis=0, concat_axis=0, tiled=True)
+    ids = route_ids.T
+    residual, outgoing = pl.pallas_call(
+        pack_body,
+        out_shape=(
+            jax.ShapeDtypeStruct((seqs, own_width), bf16),
+            jax.ShapeDtypeStruct((devices * ROW_TILE, own_width), bf16),
+        ),
+        in_specs=[IN_VMEM] * 3,
+        out_specs=(IN_VMEM, IN_VMEM),
+        name="pack",
+    )(shares, tokens, ids)
+
+    def exchange(lines):
+        split = lines.reshape(devices, ROW_TILE, own_width)
+        moved = lax.all_to_all(split, ("ep", "tp"), split_axis=0, concat_axis=0, tiled=True)
+        return moved.reshape(devices * ROW_TILE, own_width)
+
+    arrived = exchange(outgoing)
+    units = expert_gate.shape[2]
+    result = pl.pallas_call(
+        expert_body,
+        out_shape=jax.ShapeDtypeStruct((devices * ROW_TILE, own_width), bf16),
+        in_specs=[IN_VMEM] * 2 + [IN_HBM] * 3,
+        out_specs=IN_VMEM,
+        scratch_shapes=[
+            pltpu.VMEM((model_width, units), bf16),
+            pltpu.VMEM((model_width, units), bf16),
+            pltpu.VMEM((units, model_width), bf16),
+            pltpu.VMEM((ep_count * ROW_TILE, model_width), jnp.float32),
+            pltpu.SemaphoreType.DMA((3, 4)),
+        ],
+        name="expert",
+    )(arrived, ffn_gain[None], expert_gate[0], expert_up[0], expert_down[0])
+    returned = exchange(result)
+    return pl.pallas_call(
+        combine_body,
+        out_shape=jax.ShapeDtypeStruct((seqs, own_width), bf16),
+        in_specs=[IN_VMEM] * 4,
+        out_specs=IN_VMEM,
+        name="combine",
+    )(returned, residual, ids, route_weights.T)
+
+
+def local(*arrays):
+    tokens, w_gate_z, route_ids = arrays[0], arrays[2], arrays[20]
+    seqs, own_width = tokens.shape
+    width = w_gate_z.shape[1]
+    tp_count = lax.axis_size("tp")
+    expert_count = EXP_IN * lax.axis_size("ep")
+    capacity = max(2, (3 * seqs * route_ids.shape[1] + 2 * expert_count - 1) // (2 * expert_count))
+    fits = (
+        tp_count == EXP_IN
+        and capacity <= ROW_TILE
+        and seqs % ROW_TILE == 0
+        and own_width % LANES == 0
+        and width % LANES == 0
+    )
+    return (local_fast if fits else local_generic)(*arrays)
+
+
 def solution(mesh):
     in_specs = (
         P("ep", "tp"),

time: 170 us -> 72.6 us (0.43)
  waiting for transfers between devices: 65.6 us -> 0 us
  matrix products: 49.5 us -> 0 us
  blocking collectives: 19.4 us -> 50.7 us
  Pallas kernels: 0 us -> 21.4 us
  between operations: 13.7 us -> 0.02 us
  starting transfers between devices: 8.08 us -> 0 us
  local copies, waits for them, and re-layouts: 7.17 us -> 0 us
  other arithmetic: 6.07 us -> 0 us
    dot_general x12 -> x0, matrix products: 49.5 us -> none  [the longest x1 31.9 us: local(): jnp.einsum('shpn,sn->shp', new_state, query_c, precision=lax.Precision.HI...]
    reduce_scatter x2 -> x0, waiting for transfers between devices: 46.3 us -> none  [the longest x1 24 us: local(): lax.psum_scatter(partial_value, 'tp', scatter_dimension=1, tiled=True)]
    all_to_all x0 -> x3, blocking collectives: none -> 39 us  [the longest x2 29.4 us: exchange(): lax.all_to_all(split, ('ep', 'tp'), split_axis=0, concat_axis=0, tiled=True)]
    pallas_call x0 -> x4, Pallas kernels: none -> 21.4 us  [the longest x1 10.8 us: local_fast(): pl.pallas_call(mixer_body, out_shape=jax.ShapeDtypeStruct((tp_count, seqs...]
    all_to_all x2 -> x0, waiting for transfers between devices: 19.2 us -> none  [the longest x1 9.68 us: local(): lax.all_to_all(outgoing, 'ep', split_axis=0, concat_axis=0, tiled=True)]
    all_to_all x2 -> x0, starting transfers between devices: 8 us -> none  [the longest x1 4.59 us: local(): lax.all_to_all(outgoing, 'ep', split_axis=0, concat_axis=0, tiled=True)]
    all_gather x2 -> x1, blocking collectives: 19.4 us -> 11.7 us  [local_fast(): gathered = lax.all_gather(tokens, 'tp', axis=1, tiled=True)]
    convert_element_type x6 -> x0, other arithmetic: 3.91 us -> none  [the longest x1 1.43 us: local(): return (residual_own.astype(jnp.float32) + moe_share).astype(jnp.bfloat16)]
  transfers between devices with their start and end apart: 4 -> 0, of which waited for: 4 -> 0; matrix products, arithmetic and copies ran while one was open for 1% -> 0% of each run, Pallas kernels for 0% -> 0%
where the time goes in v1:
time: 72.6 us; the launch traced here: 72.1 us
  blocking collectives  50.7 us (70%)
  Pallas kernels  21.4 us (29%)
    all_to_all x2, blocking collectives, exchange(): lax.all_to_all(split, ('ep', 'tp'), split_axis=0, concat_axis=0, tiled=True)  29.4 us
    all_gather x1, blocking collectives, local_fast(): gathered = lax.all_gather(tokens, 'tp', axis=1, tiled=True)  11.7 us
    pallas_call x1, Pallas kernels, local_fast(): pl.pallas_call(mixer_body, out_shape=jax.ShapeDtypeStruct((tp_count, seqs...  10.8 us
    all_to_all x1, blocking collectives, local_fast(): lax.all_to_all(parts, 'tp', split_axis=0, concat_axis=0, tiled=True)  9.61 us
    pallas_call x1, Pallas kernels, local_fast(): pl.pallas_call(expert_body, out_shape=jax.ShapeDtypeStruct((devices * ROW...  6.65 us
    pallas_call x1, Pallas kernels, local_fast(): pl.pallas_call(pack_body, out_shape=(jax.ShapeDtypeStruct((seqs, own_widt...  1.99 us
    pallas_call x1, Pallas kernels, local_fast(): pl.pallas_call(combine_body, out_shape=jax.ShapeDtypeStruct((seqs, own_wi...  1.98 us

profile of v1, /device:TPU:0, one launch (start us, length us, event | category | flops | bytes accessed | tf_op | source)
XLA Modules:
  0.0 72.1 jit_solution(13274839429853041396)
XLA Ops:
  0.0 11.7 %all_gather.3.row_ref = bf16[48,2048]{1,0:T(8,128)(2,1)} all-gather(bf16[48,512]{1,0:T(8,128)(2,1)} %own_ref.1), channel_id=1, replica_groups=mesh['ep'=8,'tp'=4] {'tp'}, dimensions={1}, use_global_device_ids=true | all-gather | bytes 245760 | tf_op jit(solution)/shard_map/all_gather | solution.py:421
  11.7 10.8 %mixer.1 = bf16[4,48,512]{2,1,0:T(8,128)(2,1)} custom-call(bf16[48,2048]{1,0:T(8,128)(2,1)} %all_gather.3.row_ref, f32[1,2048]{1,0:T(1,128)} %bitcast.32, bf16[32,2048]{1,0:T(8,128)(2,1)} %bitcast.29, f32[1,32]{1,0:T(1,128)} %bitcast.38, f32[1,32]{1,0:T(1,128)} %bitcast.39, f32[1,32]{1,0:T(1,128)} %bitcast.40, bf16[4,512]{1,0:T(4,128)(2,1)} %tap_x_ref.1, ...), custom_call_target="tpu_custom_call" | custom-call | tf_op jit(solution)/shard_map/mixer/pallas_call | solution.py:422
  22.5 9.6 %all_to_all.15.part_ref = bf16[4,48,512]{2,1,0:T(8,128)(2,1)} all-to-all(bf16[4,48,512]{2,1,0:T(8,128)(2,1)} %mixer.1), channel_id=1, replica_groups=mesh['ep'=8,'tp'=4] {'tp'}, dimensions={0} | all-to-all | bytes 393216 | tf_op jit(solution)/shard_map/all_to_all | solution.py:460
  32.1 2.0 %pack.1 = (bf16[48,512]{1,0:T(8,128)(2,1)}, bf16[256,512]{1,0:T(8,128)(2,1)}) custom-call(bf16[4,48,512]{2,1,0:T(8,128)(2,1)} %all_to_all.15.part_ref, bf16[48,512]{1,0:T(8,128)(2,1)} %own_ref.1, s32[2,48]{1,0:T(2,128)} %bitcast.34), custom_call_target="tpu_custom_call" | custom-call | tf_op jit(solution)/shard_map/pack/pallas_call | solution.py:462
  34.1 15.2 %all_to_all.16 = bf16[32,8,512]{2,1,0:T(8,128)(2,1)} all-to-all(bf16[32,8,512]{2,1,0:T(8,128)(2,1)} %bitcast.27), channel_id=1, replica_groups=mesh['ep'=8,'tp'=4] {'ep','tp'}, dimensions={0} | all-to-all | bytes 524288 | tf_op jit(solution)/shard_map/all_to_all | solution.py:475
  49.3 6.6 %expert.1 = bf16[256,512]{1,0:T(8,128)(2,1)} custom-call(bf16[256,512]{1,0:T(8,128)(2,1)} %bitcast.24, f32[1,2048]{1,0:T(1,128)} %bitcast.33, bf16[2048,1024]{1,0:T(8,128)(2,1)} %bitcast.21, bf16[2048,1024]{1,0:T(8,128)(2,1)} %bitcast.22, bf16[1024,2048]{1,0:T(8,128)(2,1)} %bitcast.23), custom_call_target="tpu_custom_call" | custom-call | tf_op jit(solution)/shard_map/expert/pallas_call | solution.py:480
  55.9 14.2 %all_to_all.17 = bf16[32,8,512]{2,1,0:T(8,128)(2,1)} all-to-all(bf16[32,8,512]{2,1,0:T(8,128)(2,1)} %bitcast.25), channel_id=1, replica_groups=mesh['ep'=8,'tp'=4] {'ep','tp'}, dimensions={0} | all-to-all | bytes 524288 | tf_op jit(solution)/shard_map/all_to_all | solution.py:475
  70.1 2.0 %combine.1 = bf16[48,512]{1,0:T(8,128)(2,1)} custom-call(bf16[256,512]{1,0:T(8,128)(2,1)} %bitcast.26, bf16[48,512]{1,0:T(8,128)(2,1)} %get-tuple-element.8.residual_ref, s32[2,48]{1,0:T(2,128)} %bitcast.35, f32[2,48]{1,0:T(2,128)} %bitcast.37), custom_call_target="tpu_custom_call" | custom-call | tf_op jit(solution)/shard_map/combine/pallas_call | solution.py:495

commit v2 on v1

--- a/solution.py
+++ b/solution.py
@@ -202,22 +202,14 @@
     win_b_ref,
     win_c_ref,
     head_gain_ref,
-    gate_hbm,
-    value_hbm,
-    key_hbm,
-    query_hbm,
-    state_hbm,
-    out_w_hbm,
-    part_ref,
     gate_w,
     value_w,
     key_w,
     query_w,
     state,
     out_w,
+    part_ref,
     y_ref,
-    w_sems,
-    s_sems,
 ):
     tp_index = lax.axis_index("tp")
     seqs, width = y_ref.shape
@@ -225,37 +217,19 @@
     first_head = tp_index * head_count
     group = first_head // (HEADS // GROUPS)
     columns = pl.ds(pl.multiple_of(group * STATE, STATE), STATE)
-    copies = [
-        pltpu.make_async_copy(key_hbm.at[:, columns], key_w, w_sems.at[0]),
-        pltpu.make_async_copy(query_hbm.at[:, columns], query_w, w_sems.at[1]),
-        pltpu.make_async_copy(value_hbm, value_w, w_sems.at[2]),
-        pltpu.make_async_copy(gate_hbm, gate_w, w_sems.at[3]),
-        pltpu.make_async_copy(out_w_hbm, out_w, w_sems.at[4]),
-    ]
     blocks = seqs // ROW_TILE
-    state_copies = [
-        pltpu.make_async_copy(
-            state_hbm.at[pl.ds(b * ROW_TILE, ROW_TILE)], state.at[pl.ds(b * ROW_TILE, ROW_TILE)], s_sems.at[b]
-        )
-        for b in range(blocks)
-    ]
-    for copy in copies[:2] + state_copies + copies[2:]:
-        copy.start()
     rows = row_ref[...].astype(jnp.float32)
     scale = lax.rsqrt(jnp.mean(rows * rows, axis=-1, keepdims=True) + norm_epsilon)
     normed = (rows * scale * gain_ref[...]).astype(jnp.bfloat16)
     step_size = jax.nn.softplus(dot_nt(normed, step_w_ref[...]) + bias_ref[...])
     decay = jnp.exp(-step_size * jnp.exp(rate_ref[...]))
-    copies[0].wait()
-    keys = conv_rows(win_b_ref, columns, dot_bf16(normed, key_w[...]), tap_b_ref)
-    copies[1].wait()
-    queries = conv_rows(win_c_ref, columns, dot_bf16(normed, query_w[...]), tap_c_ref)
+    keys = conv_rows(win_b_ref, columns, dot_bf16(normed, key_w[:, columns]), tap_b_ref)
+    queries = conv_rows(win_c_ref, columns, dot_bf16(normed, query_w[:, columns]), tap_c_ref)
     overlap = jnp.sum(keys * queries, axis=-1, keepdims=True)
     query_hi = queries.astype(jnp.bfloat16)
     query_lo = (queries - query_hi.astype(jnp.float32)).astype(jnp.bfloat16)
     row_of = lax.broadcasted_iota(jnp.int32, (ROW_TILE, width), 0)
     for b in range(blocks):
-        state_copies[b].wait()
         lines = slice(b * ROW_TILE, (b + 1) * ROW_TILE)
         both = jnp.concatenate([query_hi[lines], query_lo[lines]], axis=0)
         total = jnp.zeros((ROW_TILE, width), jnp.float32)
@@ -267,9 +241,7 @@
         lax.broadcasted_iota(jnp.int32, (HEADS, width), 0)
         == first_head + lax.broadcasted_iota(jnp.int32, (HEADS, width), 1) // HEAD_DIM
     ).astype(jnp.float32)
-    copies[2].wait()
     values = conv_rows(win_x_ref, slice(None), dot_bf16(normed, value_w[...]), tap_x_ref)
-    copies[3].wait()
     gate_z = dot_bf16(normed, gate_w[...])
     read_out = (
         dot_exact(decay, spread) * y_ref[...]
@@ -279,7 +251,6 @@
     mean_sq = dot_nt(gated * gated, spread, lax.Precision.HIGHEST) * (1.0 / HEAD_DIM)
     scale_heads = dot_exact(lax.rsqrt(mean_sq + norm_epsilon), spread)
     mixed = (gated * scale_heads * head_gain_ref[...]).astype(jnp.bfloat16)
-    copies[4].wait()
     part_width = part_ref.shape[2]
     for j in range(part_ref.shape[0]):
         part_ref[j] = dot_bf16(mixed, out_w[:, j * part_width : (j + 1) * part_width]).astype(jnp.bfloat16)
@@ -301,38 +272,39 @@
     return jnp.logical_and(hit, rank == place), first
 
 
-def pack_body(part_ref, own_ref, ids_ref, residual_ref, outgoing_ref):
-    total = own_ref[...].astype(jnp.float32)
+def route_body(
+    own_hbm, ids_hbm, weight_hbm, own_ref, chosen_ref, high_ref, low_ref, ids_ref, weight_ref, sems
+):
+    copies = [
+        pltpu.make_async_copy(source, target, sems.at[i])
+        for i, (source, target) in enumerate(
+            ((ids_hbm, ids_ref), (weight_hbm, weight_ref), (own_hbm, own_ref))
+        )
+    ]
+    for copy in copies:
+        copy.start()
+    for copy in copies:
+        copy.wait()
+    chosen, first = slots_of(ids_ref, chosen_ref.shape[0] // ROW_TILE)
+    chosen_ref[...] = chosen.astype(jnp.bfloat16)
+    weights = weight_ref[...]
+    share = weights / jnp.sum(weights, axis=0, keepdims=True)
+    picked = jnp.where(chosen, jnp.where(first, share[0:1, :], share[1:2, :]), 0.0).T
+    high = picked.astype(jnp.bfloat16)
+    high_ref[...] = high
+    low_ref[...] = (picked - high.astype(jnp.float32)).astype(jnp.bfloat16)
+
+
+def pack_body(part_ref, own_ref, chosen_ref, residual_ref, outgoing_ref):
     share = part_ref[0].astype(jnp.float32)
     for j in range(1, part_ref.shape[0]):
         share = share + part_ref[j].astype(jnp.float32)
-    residual = (total + share).astype(jnp.bfloat16)
+    residual = (own_ref[...].astype(jnp.float32) + share).astype(jnp.bfloat16)
     residual_ref[...] = residual
-    chosen, unused = slots_of(ids_ref, outgoing_ref.shape[0] // ROW_TILE)
-    outgoing_ref[...] = dot_bf16(chosen.astype(jnp.bfloat16), residual).astype(jnp.bfloat16)
-
-
-def expert_body(
-    arrived_ref, gain_ref, gate_hbm, up_hbm, down_hbm, result_ref, gate_w, up_w, down_w, x_ref, sems
-):
-    pieces = sems.shape[1]
-    copies = []
-    for piece in range(pieces):
-        for which, (source, target) in enumerate(((gate_hbm, gate_w), (up_hbm, up_w))):
-            lines = source.shape[0] // pieces
-            span = pl.ds(piece * lines, lines)
-            copies.append(pltpu.make_async_copy(source.at[span], target.at[span], sems.at[which, piece]))
-    lines_down = down_hbm.shape[0] // pieces
-    down_copies = [
-        pltpu.make_async_copy(
-            down_hbm.at[pl.ds(piece * lines_down, lines_down)],
-            down_w.at[pl.ds(piece * lines_down, lines_down)],
-            sems.at[2, piece],
-        )
-        for piece in range(pieces)
-    ]
-    for copy in copies + down_copies:
-        copy.start()
+    outgoing_ref[...] = dot_bf16(chosen_ref[...], residual).astype(jnp.bfloat16)
+
+
+def expert_body(arrived_ref, gain_ref, gate_w, up_w, down_w, result_ref, x_ref):
     tp_count = lax.axis_size("tp")
     ep_count = lax.axis_size("ep")
     own_width = arrived_ref.shape[1]
@@ -344,21 +316,8 @@
     rows = x_ref[...]
     scale = lax.rsqrt(jnp.mean(rows * rows, axis=-1, keepdims=True) + norm_epsilon)
     ffn_in = (rows * scale * gain_ref[...]).astype(jnp.bfloat16)
-    gate_part = 0.0
-    up_part = 0.0
-    lines = gate_hbm.shape[0] // pieces
-    for piece in range(pieces):
-        span = slice(piece * lines, (piece + 1) * lines)
-        copies[2 * piece].wait()
-        gate_part = gate_part + dot_bf16(ffn_in[:, span], gate_w[span])
-        copies[2 * piece + 1].wait()
-        up_part = up_part + dot_bf16(ffn_in[:, span], up_w[span])
-    hidden = (silu(gate_part) * up_part).astype(jnp.bfloat16)
-    result = 0.0
-    for piece in range(pieces):
-        span = slice(piece * lines_down, (piece + 1) * lines_down)
-        down_copies[piece].wait()
-        result = result + dot_bf16(hidden[:, span], down_w[span])
+    hidden = (silu(dot_bf16(ffn_in, gate_w[...])) * dot_bf16(ffn_in, up_w[...])).astype(jnp.bfloat16)
+    result = dot_bf16(hidden, down_w[...])
     for source in range(ep_count):
         for part in range(tp_count):
             result_ref[pl.ds((source * tp_count + part) * ROW_TILE, ROW_TILE), :] = result[
@@ -366,22 +325,22 @@
             ].astype(jnp.bfloat16)
 
 
-def combine_body(returned_ref, residual_ref, ids_ref, weight_ref, out_ref):
-    chosen, first = slots_of(ids_ref, returned_ref.shape[0] // ROW_TILE)
-    weights = weight_ref[...]
-    share = weights / jnp.sum(weights, axis=0, keepdims=True)
-    picked = jnp.where(chosen, jnp.where(first, share[0:1, :], share[1:2, :]), 0.0)
-    high = picked.astype(jnp.bfloat16)
-    low = (picked - high.astype(jnp.float32)).astype(jnp.bfloat16)
+def combine_body(returned_ref, residual_ref, high_ref, low_ref, out_ref):
     returned = returned_ref[...]
-    dims = (((0,), (0,)), ((), ()))
-    moe_sum = lax.dot_general(high, returned, dims, preferred_element_type=jnp.float32)
-    moe_sum = moe_sum + lax.dot_general(low, returned, dims, preferred_element_type=jnp.float32)
+    moe_sum = dot_bf16(high_ref[...], returned) + dot_bf16(low_ref[...], returned)
     out_ref[...] = (residual_ref[...].astype(jnp.float32) + moe_sum).astype(jnp.bfloat16)
 
 
 IN_VMEM = pl.BlockSpec(memory_space=pltpu.VMEM)
 IN_HBM = pl.BlockSpec(memory_space=pltpu.HBM)
+
+
+def resident(array):
+    return pltpu.with_memory_space_constraint(array, pltpu.VMEM)
+
+
+def grant(mebibytes):
+    return pltpu.CompilerParams(vmem_limit_bytes=mebibytes * 2**20)
 
 
 def local_fast(
@@ -418,23 +377,40 @@
     width = w_gate_z.shape[1]
     devices = ep_count * tp_count
     bf16 = jnp.bfloat16
-    gathered = lax.all_gather(tokens, "tp", axis=1, tiled=True)
+    lines = devices * ROW_TILE
+    own, chosen, high, low = pl.pallas_call(
+        route_body,
+        out_shape=(
+            pltpu.VMEM((seqs, own_width), bf16),
+            pltpu.VMEM((lines, seqs), bf16),
+            pltpu.VMEM((seqs, lines), bf16),
+            pltpu.VMEM((seqs, lines), bf16),
+        ),
+        in_specs=[IN_HBM] * 3,
+        out_specs=(IN_VMEM,) * 4,
+        scratch_shapes=[
+            pltpu.VMEM(route_ids.shape[::-1], jnp.int32),
+            pltpu.VMEM(route_ids.shape[::-1], jnp.float32),
+            pltpu.SemaphoreType.DMA((3,)),
+        ],
+        compiler_params=grant(4),
+        cost_estimate=pl.CostEstimate(flops=2 * 10**10, bytes_accessed=2**25, transcendentals=0),
+        name="route",
+    )(
+        pltpu.with_memory_space_constraint(tokens, pltpu.HBM),
+        pltpu.with_memory_space_constraint(route_ids.T, pltpu.HBM),
+        pltpu.with_memory_space_constraint(route_weights.T, pltpu.HBM),
+    )
+    gathered = lax.all_gather(own, "tp", axis=1, tiled=True)
     parts = pl.pallas_call(
         mixer_body,
-        out_shape=jax.ShapeDtypeStruct((tp_count, seqs, own_width), bf16),
-        in_specs=[IN_VMEM] * 13 + [IN_HBM] * 6,
+        out_shape=pltpu.VMEM((tp_count, seqs, own_width), bf16),
+        in_specs=[IN_VMEM] * 19,
         out_specs=IN_VMEM,
         scratch_shapes=[
-            pltpu.VMEM((model_width, width), bf16),
-            pltpu.VMEM((model_width, width), bf16),
-            pltpu.VMEM((model_width, STATE), bf16),
-            pltpu.VMEM((model_width, STATE), bf16),
-            pltpu.VMEM((seqs, width, STATE), jnp.float32),
-            pltpu.VMEM((width, model_width), bf16),
             pltpu.VMEM((seqs, width), jnp.float32),
-            pltpu.SemaphoreType.DMA((5,)),
-            pltpu.SemaphoreType.DMA((seqs // ROW_TILE,)),
         ],
+        compiler_params=grant(4),
         name="mixer",
     )(
         gathered,
@@ -450,55 +426,54 @@
         jnp.swapaxes(window_b, 0, 1),
         jnp.swapaxes(window_c, 0, 1),
         head_gain[None],
-        w_gate_z,
-        w_value_x,
-        w_key_b,
-        w_query_c,
-        ssm_state.reshape(seqs, width, STATE),
-        w_out,
+        resident(w_gate_z),
+        resident(w_value_x),
+        resident(w_key_b),
+        resident(w_query_c),
+        resident(ssm_state.reshape(seqs, width, STATE)),
+        resident(w_out),
     )
     shares = lax.all_to_all(parts, "tp", split_axis=0, concat_axis=0, tiled=True)
-    ids = route_ids.T
     residual, outgoing = pl.pallas_call(
         pack_body,
         out_shape=(
-            jax.ShapeDtypeStruct((seqs, own_width), bf16),
-            jax.ShapeDtypeStruct((devices * ROW_TILE, own_width), bf16),
+            pltpu.VMEM((seqs, own_width), bf16),
+            pltpu.VMEM((lines, own_width), bf16),
         ),
         in_specs=[IN_VMEM] * 3,
         out_specs=(IN_VMEM, IN_VMEM),
+        compiler_params=grant(4),
         name="pack",
-    )(shares, tokens, ids)
-
-    def exchange(lines):
-        split = lines.reshape(devices, ROW_TILE, own_width)
+    )(shares, own, chosen)
+
+    def exchange(sent):
+        split = sent.reshape(devices, ROW_TILE, own_width)
         moved = lax.all_to_all(split, ("ep", "tp"), split_axis=0, concat_axis=0, tiled=True)
-        return moved.reshape(devices * ROW_TILE, own_width)
+        return moved.reshape(lines, own_width)
 
     arrived = exchange(outgoing)
-    units = expert_gate.shape[2]
     result = pl.pallas_call(
         expert_body,
-        out_shape=jax.ShapeDtypeStruct((devices * ROW_TILE, own_width), bf16),
-        in_specs=[IN_VMEM] * 2 + [IN_HBM] * 3,
+        out_shape=pltpu.VMEM((lines, own_width), bf16),
+        in_specs=[IN_VMEM] * 5,
         out_specs=IN_VMEM,
         scratch_shapes=[
-            pltpu.VMEM((model_width, units), bf16),
-            pltpu.VMEM((model_width, units), bf16),
-            pltpu.VMEM((units, model_width), bf16),
             pltpu.VMEM((ep_count * ROW_TILE, model_width), jnp.float32),
-            pltpu.SemaphoreType.DMA((3, 4)),
         ],
+        compiler_params=grant(4),
         name="expert",
-    )(arrived, ffn_gain[None], expert_gate[0], expert_up[0], expert_down[0])
+    )(
+        arrived, ffn_gain[None], resident(expert_gate[0]), resident(expert_up[0]), resident(expert_down[0])
+    )
     returned = exchange(result)
     return pl.pallas_call(
         combine_body,
         out_shape=jax.ShapeDtypeStruct((seqs, own_width), bf16),
         in_specs=[IN_VMEM] * 4,
         out_specs=IN_VMEM,
+        compiler_params=grant(4),
         name="combine",
-    )(returned, residual, ids, route_weights.T)
+    )(returned, residual, high, low)
 
 
 def local(*arrays):

time: 72.6 us -> 55.7 us (0.77)
  Pallas kernels: 21.4 us -> 8.78 us
  blocking collectives: 50.7 us -> 46.3 us
    pallas_call x3 -> x4, Pallas kernels: 19.4 us -> 7.96 us  [the longest x1 4.08 us: local_fast(): pl.pallas_call(mixer_body, out_shape=pltpu.VMEM((tp_count, seqs, own_widt...]
    all_to_all x2, blocking collectives: 29.4 us -> 27.7 us  [exchange(): lax.all_to_all(split, ('ep', 'tp'), split_axis=0, concat_axis=0, tiled=True)]
    all_to_all x1, blocking collectives: 9.61 us -> 8.11 us  [local_fast(): lax.all_to_all(parts, 'tp', split_axis=0, concat_axis=0, tiled=True)]
    all_gather x1, blocking collectives: 11.7 us -> 10.5 us  [local_fast(): gathered = lax.all_gather(own, 'tp', axis=1, tiled=True)]
    pallas_call x1, Pallas kernels: 1.98 us -> 0.82 us  [local_fast(): pl.pallas_call(combine_body, out_shape=jax.ShapeDtypeStruct((seqs, own_wi...]
where the time goes in v2:
time: 55.7 us; the launch traced here: 55.5 us
  blocking collectives  46.3 us (83%)
  Pallas kernels  8.78 us (16%)
    all_to_all x2, blocking collectives, exchange(): lax.all_to_all(split, ('ep', 'tp'), split_axis=0, concat_axis=0, tiled=True)  27.7 us
    all_gather x1, blocking collectives, local_fast(): gathered = lax.all_gather(own, 'tp', axis=1, tiled=True)  10.5 us
    all_to_all x1, blocking collectives, local_fast(): lax.all_to_all(parts, 'tp', split_axis=0, concat_axis=0, tiled=True)  8.11 us
    pallas_call x1, Pallas kernels, local_fast(): pl.pallas_call(mixer_body, out_shape=pltpu.VMEM((tp_count, seqs, own_widt...  4.08 us
    pallas_call x1, Pallas kernels, local_fast(): pl.pallas_call(expert_body, out_shape=pltpu.VMEM((lines, own_width), bf16...  2.42 us
    pallas_call x1, Pallas kernels, local_fast(): pl.pallas_call(route_body, out_shape=(pltpu.VMEM((seqs, own_width), bf16)...  1.22 us

profile of v2, /device:TPU:0, one launch (start us, length us, event | category | flops | bytes accessed | tf_op | source)
XLA Modules:
  0.0 55.5 jit_solution(13615826644527666499)
XLA Ops:
  0.0 0.0 slice-start
  0.0 0.0 slice-start.1
  0.0 0.0 slice-start.2
  0.0 0.0 copy-start.3
  0.0 0.0 copy-start.4
  0.0 0.0 copy-start.5
  0.0 0.0 copy-start.6
  0.0 0.0 copy-start.7
  0.0 0.0 copy-start.8
  0.1 0.0 copy-start.9
  0.1 0.0 copy-start.10
  0.1 0.0 copy-start.11
  0.1 0.0 copy-start.12
  0.1 0.0 copy-start.14
  0.1 0.0 copy-start.15
  0.1 0.0 copy-start.16
  0.1 0.0 copy-start.17
  0.1 0.0 copy-start.18
  0.1 0.0 copy-start.19
  0.2 0.0 copy-start.20
  0.2 1.2 %route.1 = (bf16[48,512]{1,0:T(8,128)(2,1)S(1)}, bf16[256,48]{1,0:T(8,128)(2,1)S(1)}, bf16[48,256]{1,0:T(8,128)(2,1)S(1)}, bf16[48,256]{1,0:T(8,128)(2,1)S(1)}) custom-call(bf16[48,512]{1,0:T(8,128)(2,1)} %own_hbm.1, s32[2,48]{1,0:T(2,128)} %bitcast.40, f32[2,48]{1,0:T(2,128)} %bitcast.41), custom_call_target="tpu_custom_call" | custom-call | flops 20000000000 | bytes 33554432 | tf_op jit(solution)/shard_map/route/pallas_call | solution.py:381
  1.4 10.5 %all_gather.3.row_ref = bf16[48,2048]{1,0:T(8,128)(2,1)S(1)} all-gather(bf16[48,512]{1,0:T(8,128)(2,1)S(1)} %get-tuple-element.11.own_ref), channel_id=1, replica_groups=mesh['ep'=8,'tp'=4] {'tp'}, dimensions={1}, use_global_device_ids=true | all-gather | bytes 245760 | tf_op jit(solution)/shard_map/all_gather | solution.py:404
  11.9 0.0 slice-done
  11.9 0.0 slice-done.1
  11.9 0.0 slice-done.2
  11.9 0.0 copy-done.3
  11.9 0.0 copy-done.4
  11.9 0.0 copy-done.5
  11.9 0.0 copy-done.6
  11.9 0.0 copy-done.7
  12.0 0.0 copy-done.8
  12.0 0.0 copy-done.9
  12.0 0.0 copy-done.10
  12.0 0.0 copy-done.11
  12.0 0.0 copy-done.12
  12.0 0.0 copy-done.14
  12.0 0.0 copy-done.15
  12.0 0.0 copy-done.16
  12.0 0.0 copy-done.17
  12.0 0.0 copy-done.18
  12.1 0.0 copy-done.19
  12.1 0.0 copy-done.20
  12.1 0.0 copy-start
  12.1 0.0 copy-start.1
  12.1 0.0 copy-start.2
  12.1 0.0 copy-start.13
  12.1 4.1 %mixer.1 = bf16[4,48,512]{2,1,0:T(8,128)(2,1)S(1)} custom-call(bf16[48,2048]{1,0:T(8,128)(2,1)S(1)} %all_gather.3.row_ref, f32[1,2048]{1,0:T(1,128)S(1)} %bitcast.34, bf16[32,2048]{1,0:T(8,128)(2,1)S(1)} %bitcast.31, f32[1,32]{1,0:T(1,128)S(1)} %bitcast.37, f32[1,32]{1,0:T(1,128)S(1)} %bitcast.38, f32[1,32]{1,0:T(1,128)S(1)} %bitcast.39, ...), custom_call_target="tpu_custom_call" | custom-call | tf_op jit(solution)/shard_map/mixer/pallas_call | solution.py:405
  16.2 8.1 %all_to_all.15.part_ref = bf16[4,48,512]{2,1,0:T(8,128)(2,1)S(1)} all-to-all(bf16[4,48,512]{2,1,0:T(8,128)(2,1)S(1)} %mixer.1), channel_id=1, replica_groups=mesh['ep'=8,'tp'=4] {'tp'}, dimensions={0} | all-to-all | bytes 393216 | tf_op jit(solution)/shard_map/all_to_all | solution.py:436
  24.3 0.2 pack.1
  24.6 14.9 %all_to_all.16 = bf16[32,8,512]{2,1,0:T(8,128)(2,1)S(1)} all-to-all(bf16[32,8,512]{2,1,0:T(8,128)(2,1)S(1)} %bitcast.29), channel_id=1, replica_groups=mesh['ep'=8,'tp'=4] {'ep','tp'}, dimensions={0} | all-to-all | bytes 524288 | tf_op jit(solution)/shard_map/all_to_all | solution.py:451
  39.4 0.0 copy-done
  39.4 0.0 copy-done.1
  39.4 0.0 copy-done.2
  39.5 0.0 copy-done.13
  39.5 2.4 %expert.1 = bf16[256,512]{1,0:T(8,128)(2,1)S(1)} custom-call(bf16[256,512]{1,0:T(8,128)(2,1)S(1)} %bitcast.26, f32[1,2048]{1,0:T(1,128)S(1)} %bitcast.35, bf16[2048,1024]{1,0:T(8,128)(2,1)S(1)} %bitcast.23, bf16[2048,1024]{1,0:T(8,128)(2,1)S(1)} %bitcast.24, bf16[1024,2048]{1,0:T(8,128)(2,1)S(1)} %bitcast.25), custom_call_target="tpu_custom_call" | custom-call | tf_op jit(solution)/shard_map/expert/pallas_call | solution.py:455
  41.9 12.8 %all_to_all.17 = bf16[32,8,512]{2,1,0:T(8,128)(2,1)S(1)} all-to-all(bf16[32,8,512]{2,1,0:T(8,128)(2,1)S(1)} %bitcast.27), channel_id=1, replica_groups=mesh['ep'=8,'tp'=4] {'ep','tp'}, dimensions={0} | all-to-all | bytes 524288 | tf_op jit(solution)/shard_map/all_to_all | solution.py:451
  54.7 0.8 %combine.1 = bf16[48,512]{1,0:T(8,128)(2,1)} custom-call(bf16[256,512]{1,0:T(8,128)(2,1)S(1)} %bitcast.28, bf16[48,512]{1,0:T(8,128)(2,1)S(1)} %get-tuple-element.14.residual_ref, bf16[48,256]{1,0:T(8,128)(2,1)S(1)} %get-tuple-element.15.high_ref, bf16[48,256]{1,0:T(8,128)(2,1)S(1)} %get-tuple-element.16.low_ref), custom_call_target="tpu_custom_call" | custom-call | tf_op jit(solution)/shard_map/combine/pallas_call | solution.py:469
  (1 shorter events, 0.0 us)
Async XLA Ops:
  0.0 11.9 %slice-start = ((s8[12582912]{0:T(1024)(128)(4,1)}), s8[4194304]{0:T(1024)(128)(4,1)S(1)}, s32[]{:S(2)}) async-start(s8[12582912]{0:T(1024)(128)(4,1)} %bitcast.20), calls=%async_computation.3 | async-start | bytes 8388608
  0.0 11.9 %slice-start.1 = ((s8[12582912]{0:T(1024)(128)(4,1)}), s8[4194304]{0:T(1024)(128)(4,1)S(1)}, s32[]{:S(2)}) async-start(s8[12582912]{0:T(1024)(128)(4,1)} %bitcast.20), calls=%async_computation.4 | async-start | bytes 8388608
  0.0 11.9 %slice-start.2 = ((s8[12582912]{0:T(1024)(128)(4,1)}), s8[4194304]{0:T(1024)(128)(4,1)S(1)}, s32[]{:S(2)}) async-start(s8[12582912]{0:T(1024)(128)(4,1)} %bitcast.20), calls=%async_computation.5 | async-start | bytes 8388608
  0.0 11.9 %copy-start.3 = (bf16[2048,512]{1,0:T(8,128)(2,1)S(1)}, bf16[2048,512]{1,0:T(8,128)(2,1)}, u32[]{:S(2)}) copy-start(bf16[2048,512]{1,0:T(8,128)(2,1)} %gate_w.1) | copy-start | bytes 6291460
  0.0 11.9 %copy-start.4 = (bf16[2048,512]{1,0:T(8,128)(2,1)S(1)}, bf16[2048,512]{1,0:T(8,128)(2,1)}, u32[]{:S(2)}) copy-start(bf16[2048,512]{1,0:T(8,128)(2,1)} %value_w.1) | copy-start | bytes 6291460
  0.0 11.9 %copy-start.5 = (bf16[512,2048]{1,0:T(8,128)(2,1)S(1)}, bf16[512,2048]{1,0:T(8,128)(2,1)}, u32[]{:S(2)}) copy-start(bf16[512,2048]{1,0:T(8,128)(2,1)} %out_w.1) | copy-start | bytes 6291460
  0.0 11.9 %copy-start.6 = (bf16[2048,256]{1,0:T(8,128)(2,1)S(1)}, bf16[2048,256]{1,0:T(8,128)(2,1)}, u32[]{:S(2)}) copy-start(bf16[2048,256]{1,0:T(8,128)(2,1)} %key_w.1) | copy-start | bytes 3145732
  0.0 11.9 %copy-start.7 = (bf16[2048,256]{1,0:T(8,128)(2,1)S(1)}, bf16[2048,256]{1,0:T(8,128)(2,1)}, u32[]{:S(2)}) copy-start(bf16[2048,256]{1,0:T(8,128)(2,1)} %query_w.1) | copy-start | bytes 3145732
  0.0 11.9 %copy-start.8 = (bf16[48,3,512]{2,0,1:T(8,128)(2,1)S(1)}, bf16[48,3,512]{2,0,1:T(8,128)(2,1)}, u32[]{:S(2)}) copy-start(bf16[48,3,512]{2,0,1:T(8,128)(2,1)} %param.38) | copy-start | bytes 442372
  0.1 11.9 %copy-start.9 = (bf16[2048,32]{0,1:T(8,128)(2,1)S(1)}, bf16[2048,32]{0,1:T(8,128)(2,1)}, u32[]{:S(2)}) copy-start(bf16[2048,32]{0,1:T(8,128)(2,1)} %param.31) | copy-start | bytes 393220
  0.1 11.9 %copy-start.10 = (bf16[48,3,256]{2,0,1:T(8,128)(2,1)S(1)}, bf16[48,3,256]{2,0,1:T(8,128)(2,1)}, u32[]{:S(2)}) copy-start(bf16[48,3,256]{2,0,1:T(8,128)(2,1)} %param.39) | copy-start | bytes 221188
  0.1 11.9 %copy-start.11 = (bf16[48,3,256]{2,0,1:T(8,128)(2,1)S(1)}, bf16[48,3,256]{2,0,1:T(8,128)(2,1)}, u32[]{:S(2)}) copy-start(bf16[48,3,256]{2,0,1:T(8,128)(2,1)} %param.40) | copy-start | bytes 221188
  0.1 11.9 %copy-start.12 = (f32[2048]{0:T(1024)S(1)}, f32[2048]{0:T(1024)}, u32[]{:S(2)}) copy-start(f32[2048]{0:T(1024)} %param.26) | copy-start | bytes 24580
  0.1 11.9 %copy-start.14 = (bf16[4,512]{1,0:T(4,128)(2,1)S(1)}, bf16[4,512]{1,0:T(4,128)(2,1)}, u32[]{:S(2)}) copy-start(bf16[4,512]{1,0:T(4,128)(2,1)} %tap_x_ref.1) | copy-start | bytes 12292
  0.1 11.9 %copy-start.15 = (bf16[4,256]{1,0:T(4,128)(2,1)S(1)}, bf16[4,256]{1,0:T(4,128)(2,1)}, u32[]{:S(2)}) copy-start(bf16[4,256]{1,0:T(4,128)(2,1)} %tap_b_ref.1) | copy-start | bytes 6148
  0.1 11.9 %copy-start.16 = (bf16[4,256]{1,0:T(4,128)(2,1)S(1)}, bf16[4,256]{1,0:T(4,128)(2,1)}, u32[]{:S(2)}) copy-start(bf16[4,256]{1,0:T(4,128)(2,1)} %tap_c_ref.1) | copy-start | bytes 6148
  0.1 11.9 %copy-start.17 = (f32[512]{0:T(512)S(1)}, f32[512]{0:T(512)}, u32[]{:S(2)}) copy-start(f32[512]{0:T(512)} %param.42) | copy-start | bytes 6148
  0.1 11.9 %copy-start.18 = (f32[32]{0:T(128)S(1)}, f32[32]{0:T(128)}, u32[]{:S(2)}) copy-start(f32[32]{0:T(128)} %param.32) | copy-start | bytes 388
  0.1 11.9 %copy-start.19 = (f32[32]{0:T(128)S(1)}, f32[32]{0:T(128)}, u32[]{:S(2)}) copy-start(f32[32]{0:T(128)} %param.33) | copy-start | bytes 388
  0.2 11.9 %copy-start.20 = (f32[32]{0:T(128)S(1)}, f32[32]{0:T(128)}, u32[]{:S(2)}) copy-start(f32[32]{0:T(128)} %param.34) | copy-start | bytes 388
  12.1 27.4 %copy-start = (bf16[1,2048,1024]{2,1,0:T(8,128)(2,1)S(1)}, bf16[1,2048,1024]{2,1,0:T(8,128)(2,1)}, u32[]{:S(2)}) copy-start(bf16[1,2048,1024]{2,1,0:T(8,128)(2,1)} %param.47) | copy-start | bytes 12582916
  12.1 27.4 %copy-start.1 = (bf16[1,2048,1024]{2,1,0:T(8,128)(2,1)S(1)}, bf16[1,2048,1024]{2,1,0:T(8,128)(2,1)}, u32[]{:S(2)}) copy-start(bf16[1,2048,1024]{2,1,0:T(8,128)(2,1)} %param.48) | copy-start | bytes 12582916
  12.1 27.3 %copy-start.2 = (bf16[1,1024,2048]{2,1,0:T(8,128)(2,1)S(1)}, bf16[1,1024,2048]{2,1,0:T(8,128)(2,1)}, u32[]{:S(2)}) copy-start(bf16[1,1024,2048]{2,1,0:T(8,128)(2,1)} %param.49) | copy-start | bytes 12582916
  12.1 27.3 %copy-start.13 = (f32[2048]{0:T(1024)S(1)}, f32[2048]{0:T(1024)}, u32[]{:S(2)}) copy-start(f32[2048]{0:T(1024)} %param.44) | copy-start | bytes 24580

commit v3 on v2

--- a/solution.py
+++ b/solution.py
@@ -189,7 +189,8 @@
 
 
 def mixer_body(
-    row_ref,
+    own_ref,
+    piece_refs,
     gain_ref,
     step_w_ref,
     bias_ref,
@@ -208,8 +209,9 @@
     query_w,
     state,
     out_w,
-    part_ref,
+    part_refs,
     y_ref,
+    row_ref,
 ):
     tp_index = lax.axis_index("tp")
     seqs, width = y_ref.shape
@@ -218,6 +220,9 @@
     group = first_head // (HEADS // GROUPS)
     columns = pl.ds(pl.multiple_of(group * STATE, STATE), STATE)
     blocks = seqs // ROW_TILE
+    own_width = own_ref.shape[1]
+    for k, piece_ref in enumerate((own_ref, *piece_refs)):
+        row_ref[:, pl.ds(pl.multiple_of((tp_index ^ k) * own_width, own_width), own_width)] = piece_ref[...]
     rows = row_ref[...].astype(jnp.float32)
     scale = lax.rsqrt(jnp.mean(rows * rows, axis=-1, keepdims=True) + norm_epsilon)
     normed = (rows * scale * gain_ref[...]).astype(jnp.bfloat16)
@@ -251,16 +256,15 @@
     mean_sq = dot_nt(gated * gated, spread, lax.Precision.HIGHEST) * (1.0 / HEAD_DIM)
     scale_heads = dot_exact(lax.rsqrt(mean_sq + norm_epsilon), spread)
     mixed = (gated * scale_heads * head_gain_ref[...]).astype(jnp.bfloat16)
-    part_width = part_ref.shape[2]
-    for j in range(part_ref.shape[0]):
-        part_ref[j] = dot_bf16(mixed, out_w[:, j * part_width : (j + 1) * part_width]).astype(jnp.bfloat16)
-
-
-def slots_of(ids_ref, experts):
+    for k, part_ref in enumerate(part_refs):
+        span = pl.ds(pl.multiple_of((tp_index ^ k) * own_width, own_width), own_width)
+        part_ref[...] = dot_bf16(mixed, out_w[:, span]).astype(part_ref.dtype)
+
+
+def slots_of(ids_ref, experts, lines):
     seqs = ids_ref.shape[1]
-    shape = (experts * ROW_TILE, seqs)
-    line = lax.broadcasted_iota(jnp.int32, shape, 0)
-    expert = line // ROW_TILE
+    line = lax.broadcasted_iota(jnp.int32, (lines, seqs), 0)
+    expert = line % experts
     first = ids_ref[0:1, :] == expert
     second = ids_ref[1:2, :] == expert
     hit = jnp.logical_or(first, second)
@@ -268,24 +272,19 @@
         lax.broadcasted_iota(jnp.int32, (seqs, seqs), 0) < lax.broadcasted_iota(jnp.int32, (seqs, seqs), 1)
     ).astype(jnp.bfloat16)
     rank = dot_bf16(hit.astype(jnp.bfloat16), before)
-    place = (line % ROW_TILE).astype(jnp.float32)
+    place = (line // experts).astype(jnp.float32)
     return jnp.logical_and(hit, rank == place), first
 
 
-def route_body(
-    own_hbm, ids_hbm, weight_hbm, own_ref, chosen_ref, high_ref, low_ref, ids_ref, weight_ref, sems
-):
-    copies = [
-        pltpu.make_async_copy(source, target, sems.at[i])
-        for i, (source, target) in enumerate(
-            ((ids_hbm, ids_ref), (weight_hbm, weight_ref), (own_hbm, own_ref))
-        )
-    ]
-    for copy in copies:
-        copy.start()
-    for copy in copies:
-        copy.wait()
-    chosen, first = slots_of(ids_ref, chosen_ref.shape[0] // ROW_TILE)
+def entry_body(own_hbm, own_ref, sem):
+    copy = pltpu.make_async_copy(own_hbm, own_ref, sem)
+    copy.start()
+    copy.wait()
+
+
+def route_body(ids_ref, weight_ref, chosen_ref, high_ref, low_ref):
+    experts = EXP_IN * lax.axis_size("ep")
+    chosen, first = slots_of(ids_ref, experts, chosen_ref.shape[0])
     chosen_ref[...] = chosen.astype(jnp.bfloat16)
     weights = weight_ref[...]
     share = weights / jnp.sum(weights, axis=0, keepdims=True)
@@ -295,40 +294,83 @@
     low_ref[...] = (picked - high.astype(jnp.float32)).astype(jnp.bfloat16)
 
 
-def pack_body(part_ref, own_ref, chosen_ref, residual_ref, outgoing_ref):
-    share = part_ref[0].astype(jnp.float32)
-    for j in range(1, part_ref.shape[0]):
-        share = share + part_ref[j].astype(jnp.float32)
-    residual = (own_ref[...].astype(jnp.float32) + share).astype(jnp.bfloat16)
+def write_blocks(line_ref, moved_ref):
+    devices, blocks, width = moved_ref.shape
+    for d in range(devices):
+        for k in range(width // LANES):
+            moved_ref[d, :, k * LANES : (k + 1) * LANES] = line_ref[
+                k, d * blocks : (d + 1) * blocks
+            ].astype(moved_ref.dtype)
+
+
+def read_blocks(moved_ref, line_ref):
+    devices, blocks, width = moved_ref.shape
+    for d in range(devices):
+        for k in range(width // LANES):
+            line_ref[k, d * blocks : (d + 1) * blocks] = moved_ref[
+                d, :, k * LANES : (k + 1) * LANES
+            ].astype(line_ref.dtype)
+
+
+def pack_body(own_ref, part_refs, chosen_ref, residual_ref, outgoing_ref, line_ref):
+    share = own_ref[...].astype(jnp.float32)
+    for part_ref in part_refs:
+        share = share + part_ref[...].astype(jnp.float32)
+    residual = share.astype(jnp.bfloat16)
     residual_ref[...] = residual
-    outgoing_ref[...] = dot_bf16(chosen_ref[...], residual).astype(jnp.bfloat16)
-
-
-def expert_body(arrived_ref, gain_ref, gate_w, up_w, down_w, result_ref, x_ref):
+    rows = dot_bf16(chosen_ref[...], residual)
+    devices, blocks, width = outgoing_ref.shape
+    for k in range(width // LANES):
+        for j in range(blocks):
+            line_ref[k, pl.ds(j, devices, stride=blocks)] = rows[
+                k * devices : (k + 1) * devices, j * LANES : (j + 1) * LANES
+            ]
+    write_blocks(line_ref, outgoing_ref)
+
+
+def expert_body(arrived_ref, gain_ref, gate_w, up_w, down_w, result_ref, x_ref, line_ref):
     tp_count = lax.axis_size("tp")
     ep_count = lax.axis_size("ep")
-    own_width = arrived_ref.shape[1]
-    for source in range(ep_count):
-        for part in range(tp_count):
-            x_ref[source * ROW_TILE : (source + 1) * ROW_TILE, part * own_width : (part + 1) * own_width] = (
-                arrived_ref[pl.ds((source * tp_count + part) * ROW_TILE, ROW_TILE), :].astype(jnp.float32)
-            )
+    devices, blocks, width = arrived_ref.shape
+    own_width = blocks * LANES
+    read_blocks(arrived_ref, line_ref)
+    places = [
+        (
+            slice(k * ep_count, (k + 1) * ep_count),
+            slice(part * own_width + j * LANES, part * own_width + (j + 1) * LANES),
+            pl.ds(part * blocks + j, ep_count, stride=tp_count * blocks),
+            k,
+        )
+        for k in range(width // LANES)
+        for part in range(tp_count)
+        for j in range(blocks)
+    ]
+    for row, column, line, k in places:
+        x_ref[row, column] = line_ref[k, line]
     rows = x_ref[...]
     scale = lax.rsqrt(jnp.mean(rows * rows, axis=-1, keepdims=True) + norm_epsilon)
     ffn_in = (rows * scale * gain_ref[...]).astype(jnp.bfloat16)
     hidden = (silu(dot_bf16(ffn_in, gate_w[...])) * dot_bf16(ffn_in, up_w[...])).astype(jnp.bfloat16)
     result = dot_bf16(hidden, down_w[...])
-    for source in range(ep_count):
-        for part in range(tp_count):
-            result_ref[pl.ds((source * tp_count + part) * ROW_TILE, ROW_TILE), :] = result[
-                source * ROW_TILE : (source + 1) * ROW_TILE, part * own_width : (part + 1) * own_width
-            ].astype(jnp.bfloat16)
-
-
-def combine_body(returned_ref, residual_ref, high_ref, low_ref, out_ref):
-    returned = returned_ref[...]
-    moe_sum = dot_bf16(high_ref[...], returned) + dot_bf16(low_ref[...], returned)
-    out_ref[...] = (residual_ref[...].astype(jnp.float32) + moe_sum).astype(jnp.bfloat16)
+    for row, column, line, k in places:
+        line_ref[k, line] = result[row, column]
+    write_blocks(line_ref, result_ref)
+
+
+def combine_body(returned_ref, residual_ref, high_ref, low_ref, out_ref, line_ref):
+    devices, blocks, width = returned_ref.shape
+    read_blocks(returned_ref, line_ref)
+    for j in range(blocks):
+        rows = jnp.concatenate(
+            [
+                line_ref[k, pl.ds(j, devices, stride=blocks)]
+                for k in range(width // LANES)
+            ],
+            axis=0,
+        ).astype(jnp.bfloat16)
+        moe_sum = dot_bf16(high_ref[...], rows) + dot_bf16(low_ref[...], rows)
+        span = slice(j * LANES, (j + 1) * LANES)
+        out_ref[:, span] = (residual_ref[:, span].astype(jnp.float32) + moe_sum).astype(jnp.bfloat16)
 
 
 IN_VMEM = pl.BlockSpec(memory_space=pltpu.VMEM)
@@ -377,43 +419,56 @@
     width = w_gate_z.shape[1]
     devices = ep_count * tp_count
     bf16 = jnp.bfloat16
-    lines = devices * ROW_TILE
-    own, chosen, high, low = pl.pallas_call(
+    f32 = jnp.float32
+    capacity = capacity_of(seqs, route_ids.shape[1], devices)
+    blocks = own_width // LANES
+    lines = devices * capacity
+    moved_shape = (devices, blocks, capacity * LANES)
+    line_scratch = pltpu.VMEM((capacity, devices * blocks, LANES), f32)
+
+    def shift(array, k):
+        return lax.ppermute(array, "tp", [(i, i ^ k) for i in range(tp_count)])
+
+    own = pl.pallas_call(
+        entry_body,
+        out_shape=pltpu.VMEM((seqs, own_width), bf16),
+        in_specs=[IN_HBM],
+        out_specs=IN_VMEM,
+        scratch_shapes=[pltpu.SemaphoreType.DMA],
+        compiler_params=grant(4),
+        cost_estimate=pl.CostEstimate(flops=2 * 10**10, bytes_accessed=2**25, transcendentals=0),
+        name="entry",
+    )(pltpu.with_memory_space_constraint(tokens, pltpu.HBM))
+    pieces = tuple(shift(own, k) for k in range(1, tp_count))
+    chosen, high, low = pl.pallas_call(
         route_body,
         out_shape=(
-            pltpu.VMEM((seqs, own_width), bf16),
             pltpu.VMEM((lines, seqs), bf16),
             pltpu.VMEM((seqs, lines), bf16),
             pltpu.VMEM((seqs, lines), bf16),
         ),
-        in_specs=[IN_HBM] * 3,
-        out_specs=(IN_VMEM,) * 4,
+        in_specs=[IN_VMEM] * 2,
+        out_specs=(IN_VMEM,) * 3,
+        compiler_params=grant(4),
+        cost_estimate=pl.CostEstimate(flops=10**10, bytes_accessed=2**24, transcendentals=0),
+        name="route",
+    )(route_ids.T, route_weights.T)
+    (parts,) = pl.pallas_call(
+        mixer_body,
+        out_shape=(
+            (pltpu.VMEM((seqs, own_width), f32),) + (pltpu.VMEM((seqs, own_width), bf16),) * (tp_count - 1),
+        ),
+        in_specs=[IN_VMEM, (IN_VMEM,) * (tp_count - 1)] + [IN_VMEM] * 18,
+        out_specs=((IN_VMEM,) * tp_count,),
         scratch_shapes=[
-            pltpu.VMEM(route_ids.shape[::-1], jnp.int32),
-            pltpu.VMEM(route_ids.shape[::-1], jnp.float32),
-            pltpu.SemaphoreType.DMA((3,)),
-        ],
-        compiler_params=grant(4),
-        cost_estimate=pl.CostEstimate(flops=2 * 10**10, bytes_accessed=2**25, transcendentals=0),
-        name="route",
-    )(
-        pltpu.with_memory_space_constraint(tokens, pltpu.HBM),
-        pltpu.with_memory_space_constraint(route_ids.T, pltpu.HBM),
-        pltpu.with_memory_space_constraint(route_weights.T, pltpu.HBM),
-    )
-    gathered = lax.all_gather(own, "tp", axis=1, tiled=True)
-    parts = pl.pallas_call(
-        mixer_body,
-        out_shape=pltpu.VMEM((tp_count, seqs, own_width), bf16),
-        in_specs=[IN_VMEM] * 19,
-        out_specs=IN_VMEM,
-        scratch_shapes=[
-            pltpu.VMEM((seqs, width), jnp.float32),
+            pltpu.VMEM((seqs, width), f32),
+            pltpu.VMEM((seqs, model_width), bf16),
         ],
         compiler_params=grant(4),
         name="mixer",
     )(
-        gathered,
+        own,
+        pieces,
         mix_gain[None],
         w_step.T,
         step_bias[None],
@@ -433,59 +488,58 @@
         resident(ssm_state.reshape(seqs, width, STATE)),
         resident(w_out),
     )
-    shares = lax.all_to_all(parts, "tp", split_axis=0, concat_axis=0, tiled=True)
+    shares = (parts[0],) + tuple(shift(parts[k], k) for k in range(1, tp_count))
     residual, outgoing = pl.pallas_call(
         pack_body,
-        out_shape=(
-            pltpu.VMEM((seqs, own_width), bf16),
-            pltpu.VMEM((lines, own_width), bf16),
-        ),
-        in_specs=[IN_VMEM] * 3,
+        out_shape=(pltpu.VMEM((seqs, own_width), bf16), pltpu.VMEM(moved_shape, bf16)),
+        in_specs=[IN_VMEM, (IN_VMEM,) * tp_count, IN_VMEM],
         out_specs=(IN_VMEM, IN_VMEM),
+        scratch_shapes=[line_scratch],
         compiler_params=grant(4),
         name="pack",
-    )(shares, own, chosen)
+    )(own, shares, chosen)
 
     def exchange(sent):
-        split = sent.reshape(devices, ROW_TILE, own_width)
-        moved = lax.all_to_all(split, ("ep", "tp"), split_axis=0, concat_axis=0, tiled=True)
-        return moved.reshape(lines, own_width)
-
-    arrived = exchange(outgoing)
+        return lax.all_to_all(sent, ("ep", "tp"), split_axis=0, concat_axis=0, tiled=True)
+
     result = pl.pallas_call(
         expert_body,
-        out_shape=pltpu.VMEM((lines, own_width), bf16),
+        out_shape=pltpu.VMEM(moved_shape, bf16),
         in_specs=[IN_VMEM] * 5,
         out_specs=IN_VMEM,
-        scratch_shapes=[
-            pltpu.VMEM((ep_count * ROW_TILE, model_width), jnp.float32),
-        ],
+        scratch_shapes=[pltpu.VMEM((ep_count * capacity, model_width), f32), line_scratch],
         compiler_params=grant(4),
         name="expert",
     )(
-        arrived, ffn_gain[None], resident(expert_gate[0]), resident(expert_up[0]), resident(expert_down[0])
-    )
-    returned = exchange(result)
+        exchange(outgoing),
+        ffn_gain[None],
+        resident(expert_gate[0]),
+        resident(expert_up[0]),
+        resident(expert_down[0]),
+    )
     return pl.pallas_call(
         combine_body,
         out_shape=jax.ShapeDtypeStruct((seqs, own_width), bf16),
         in_specs=[IN_VMEM] * 4,
         out_specs=IN_VMEM,
+        scratch_shapes=[line_scratch],
         compiler_params=grant(4),
         name="combine",
-    )(returned, residual, high, low)
+    )(exchange(result), residual, high, low)
+
+
+def capacity_of(seqs, top_count, experts):
+    return max(2, (3 * seqs * top_count + 2 * experts - 1) // (2 * experts))
 
 
 def local(*arrays):
-    tokens, w_gate_z, route_ids = arrays[0], arrays[2], arrays[20]
+    tokens, w_gate_z = arrays[0], arrays[2]
     seqs, own_width = tokens.shape
     width = w_gate_z.shape[1]
     tp_count = lax.axis_size("tp")
-    expert_count = EXP_IN * lax.axis_size("ep")
-    capacity = max(2, (3 * seqs * route_ids.shape[1] + 2 * expert_count - 1) // (2 * expert_count))
     fits = (
         tp_count == EXP_IN
-        and capacity <= ROW_TILE
+        and lax.axis_size("ep") % ROW_TILE == 0
         and seqs % ROW_TILE == 0
         and own_width % LANES == 0
         and width % LANES == 0

time: 55.7 us -> 49.3 us (0.89)
  blocking collectives: 46.3 us -> 24.2 us
  starting transfers between devices: 0 us -> 8.2 us
  waiting for transfers between devices: 0 us -> 7.25 us
    all_to_all x3 -> x2, blocking collectives: 35.8 us -> 24.2 us  [exchange(): lax.all_to_all(sent, ('ep', 'tp'), split_axis=0, concat_axis=0, tiled=True)]
    all_gather x1 -> x0, blocking collectives: 10.5 us -> none  [local_fast(): gathered = lax.all_gather(own, 'tp', axis=1, tiled=True)]
    ppermute x0 -> x6, starting transfers between devices: none -> 8.2 us  [shift(): return lax.ppermute(array, 'tp', [(i, i ^ k) for i in range(tp_count)])]
    ppermute x0 -> x6, waiting for transfers between devices: none -> 7.25 us  [shift(): return lax.ppermute(array, 'tp', [(i, i ^ k) for i in range(tp_count)])]
    pallas_call x3 -> x4, Pallas kernels: 7.72 us -> 7.87 us  [the longest x1 4.12 us: local_fast(): pl.pallas_call(mixer_body, out_shape=((pltpu.VMEM((seqs, own_width), f32)...]
  transfers between devices with their start and end apart: 0 -> 6, of which waited for: 0 -> 5; matrix products, arithmetic and copies ran while one was open for 0% -> 0% of each run, Pallas kernels for 0% -> 0%
where the time goes in v3:
time: 49.3 us; the launch traced here: 49.1 us
  blocking collectives  24.2 us (49%)
  Pallas kernels  9.01 us (18%)
  starting transfers between devices  8.2 us (17%)
  waiting for transfers between devices  7.25 us (15%)
    all_to_all x2, blocking collectives, exchange(): lax.all_to_all(sent, ('ep', 'tp'), split_axis=0, concat_axis=0, tiled=True)  24.2 us
    ppermute x6, starting transfers between devices, shift(): return lax.ppermute(array, 'tp', [(i, i ^ k) for i in range(tp_count)])  8.2 us
    ppermute x6, waiting for transfers between devices, shift(): return lax.ppermute(array, 'tp', [(i, i ^ k) for i in range(tp_count)])  7.25 us
    pallas_call x1, Pallas kernels, local_fast(): pl.pallas_call(mixer_body, out_shape=((pltpu.VMEM((seqs, own_width), f32)...  4.12 us
    pallas_call x1, Pallas kernels, local_fast(): pl.pallas_call(expert_body, out_shape=pltpu.VMEM(moved_shape, bf16), in_s...  2.58 us
  transfers between devices with their start and end apart: 6, of which 5 were waited for; matrix products, arithmetic and copies ran while one was open for 0% of the time, Pallas kernels for 0%

profile of v3, /device:TPU:0, one launch (start us, length us, event | category | flops | bytes accessed | tf_op | source)
XLA Modules:
  0.0 49.1 jit_solution(9213956433204378438)
XLA Ops:
  0.0 0.0 copy-start.6
  0.0 0.0 copy-start.18
  0.0 0.0 copy-start.12
  0.0 0.0 copy-start.17
  0.0 0.0 copy-start.16
  0.0 0.0 copy-start.15
  0.0 0.0 copy-start.21
  0.1 0.0 copy-start.20
  0.1 0.0 copy-start.19
  0.1 0.0 copy-start.10
  0.1 0.0 copy-start.8
  0.1 0.0 copy-start.7
  0.1 0.0 copy-start.5
  0.1 0.0 copy-start.4
  0.1 0.0 copy-start.13
  0.1 0.0 copy-start
  0.1 1.0 %entry.1.own_ref = bf16[48,512]{1,0:T(8,128)(2,1)S(1)} custom-call(bf16[48,512]{1,0:T(8,128)(2,1)} %own_hbm.1), custom_call_target="tpu_custom_call" | custom-call | flops 20000000000 | bytes 33554432 | tf_op jit(solution)/shard_map/entry/pallas_call | solution.py:432
  1.1 4.0 %collective-permute-start.2 = (bf16[48,512]{1,0:T(8,128)(2,1)S(1)}, bf16[48,512]{1,0:T(8,128)(2,1)S(1)}, u32[]{:S(2)}, u32[]{:S(2)}) collective-permute-start(bf16[48,512]{1,0:T(8,128)(2,1)S(1)} %entry.1.own_ref), channel_id=1, source_target_pairs={{0,3},{1,2},{2,1},{3,0},{4,7},{5,6},{6,5},{7,4},{8,11},{9,10},{10,... | collective-permute-start | bytes 147464 | tf_op jit(solution)/shard_map/ppermute | solution.py:430
  5.1 0.5 %collective-permute-start.1 = (bf16[48,512]{1,0:T(8,128)(2,1)S(1)}, bf16[48,512]{1,0:T(8,128)(2,1)S(1)}, u32[]{:S(2)}, u32[]{:S(2)}) collective-permute-start(bf16[48,512]{1,0:T(8,128)(2,1)S(1)} %entry.1.own_ref), channel_id=1, source_target_pairs={{0,2},{1,3},{2,0},{3,1},{4,6},{5,7},{6,4},{7,5},{8,10},{9,11},{10,... | collective-permute-start | bytes 147464 | tf_op jit(solution)/shard_map/ppermute | solution.py:430
  5.6 0.1 collective-permute-start
  5.8 1.4 %collective-permute-done.2.piece_refs_2_ = bf16[48,512]{1,0:T(8,128)(2,1)S(1)} collective-permute-done((bf16[48,512]{1,0:T(8,128)(2,1)S(1)}, bf16[48,512]{1,0:T(8,128)(2,1)S(1)}, u32[]{:S(2)}, u32[]{:S(2)}) %collective-permute-start.2) | collective-permute-done | bytes 49184 | tf_op jit(solution)/shard_map/ppermute | solution.py:430
  7.2 2.0 %collective-permute-done.1.piece_refs_1_ = bf16[48,512]{1,0:T(8,128)(2,1)S(1)} collective-permute-done((bf16[48,512]{1,0:T(8,128)(2,1)S(1)}, bf16[48,512]{1,0:T(8,128)(2,1)S(1)}, u32[]{:S(2)}, u32[]{:S(2)}) %collective-permute-start.1) | collective-permute-done | bytes 49184 | tf_op jit(solution)/shard_map/ppermute | solution.py:430
  9.2 0.5 %collective-permute-done.piece_refs_0_ = bf16[48,512]{1,0:T(8,128)(2,1)S(1)} collective-permute-done((bf16[48,512]{1,0:T(8,128)(2,1)S(1)}, bf16[48,512]{1,0:T(8,128)(2,1)S(1)}, u32[]{:S(2)}, u32[]{:S(2)}) %collective-permute-start) | collective-permute-done | bytes 49184 | tf_op jit(solution)/shard_map/ppermute | solution.py:430
  9.7 0.0 copy-done.6
  9.7 0.0 copy-done.18
  9.7 0.0 copy-done.12
  9.7 0.0 copy-done.11
  9.7 0.0 copy-done.9
  9.7 0.0 copy-done.17
  9.8 0.0 copy-done.16
  9.8 0.0 copy-done.15
  9.8 0.0 copy-done.21
  9.8 0.0 copy-done.20
  9.8 0.0 copy-done.19
  9.8 0.0 copy-done.10
  9.8 0.0 copy-done.8
  9.8 0.0 copy-done.7
  9.8 0.0 copy-done.5
  9.8 0.0 copy-done.4
  9.9 0.0 copy-done.13
  9.9 0.0 copy-done
  9.9 0.0 copy-start.22
  9.9 0.0 copy-start.23
  9.9 4.1 %mixer.1 = (f32[48,512]{1,0:T(8,128)S(1)}, bf16[48,512]{1,0:T(8,128)(2,1)S(1)}, bf16[48,512]{1,0:T(8,128)(2,1)S(1)}, bf16[48,512]{1,0:T(8,128)(2,1)S(1)}) custom-call(bf16[48,512]{1,0:T(8,128)(2,1)S(1)} %entry.1.own_ref, bf16[48,512]{1,0:T(8,128)(2,1)S(1)} %collective-permute-done.piece_refs_0_, bf16[48,512]{1,0:T(8,128)(2,1)S(1)} %collective-permute-done.1.piece_refs_1_, ...), custom_call_target="tpu_custom_call" | custom-call | tf_op jit(solution)/shard_map/mixer/pallas_call | solution.py:456
  14.0 0.4 collective-permute-start.3
  14.4 1.7 %collective-permute-start.4 = (bf16[48,512]{1,0:T(8,128)(2,1)S(1)}, bf16[48,512]{1,0:T(8,128)(2,1)S(1)}, u32[]{:S(2)}, u32[]{:S(2)}) collective-permute-start(bf16[48,512]{1,0:T(8,128)(2,1)S(1)} %get-tuple-element.16), channel_id=1, source_target_pairs={{0,2},{1,3},{2,0},{3,1},{4,6},{5,7},{6,4},{7,5},{8,10},{9,11},{10,... | collective-permute-start | bytes 147464 | tf_op jit(solution)/shard_map/ppermute | solution.py:430
  16.1 1.4 %collective-permute-start.5 = (bf16[48,512]{1,0:T(8,128)(2,1)S(1)}, bf16[48,512]{1,0:T(8,128)(2,1)S(1)}, u32[]{:S(2)}, u32[]{:S(2)}) collective-permute-start(bf16[48,512]{1,0:T(8,128)(2,1)S(1)} %get-tuple-element.17), channel_id=1, source_target_pairs={{0,3},{1,2},{2,1},{3,0},{4,7},{5,6},{6,5},{7,4},{8,11},{9,10},{10,... | collective-permute-start | bytes 147464 | tf_op jit(solution)/shard_map/ppermute | solution.py:430
  17.6 0.0 copy-done.22
  17.6 0.0 copy-done.23
  17.6 0.0 copy-start.3
  17.6 0.0 copy-start.14
  17.6 0.2 route.1
  17.8 0.7 %collective-permute-done.3.part_refs_1_ = bf16[48,512]{1,0:T(8,128)(2,1)S(1)} collective-permute-done((bf16[48,512]{1,0:T(8,128)(2,1)S(1)}, bf16[48,512]{1,0:T(8,128)(2,1)S(1)}, u32[]{:S(2)}, u32[]{:S(2)}) %collective-permute-start.3) | collective-permute-done | bytes 49184 | tf_op jit(solution)/shard_map/ppermute | solution.py:430
  18.6 0.0 collective-permute-done.4.part_refs_2_
  18.6 2.6 %collective-permute-done.5.part_refs_3_ = bf16[48,512]{1,0:T(8,128)(2,1)S(1)} collective-permute-done((bf16[48,512]{1,0:T(8,128)(2,1)S(1)}, bf16[48,512]{1,0:T(8,128)(2,1)S(1)}, u32[]{:S(2)}, u32[]{:S(2)}) %collective-permute-start.5) | collective-permute-done | bytes 49184 | tf_op jit(solution)/shard_map/ppermute | solution.py:430
  21.1 0.2 pack.1
  21.4 13.5 %all_to_all.10.arrived_ref = bf16[32,4,640]{2,1,0:T(4,128)(2,1)S(1)} all-to-all(bf16[32,4,640]{2,1,0:T(4,128)(2,1)S(1)} %get-tuple-element.19), channel_id=1, replica_groups=mesh['ep'=8,'tp'=4] {'ep','tp'}, dimensions={0} | all-to-all | bytes 327680 | tf_op jit(solution)/shard_map/all_to_all | solution.py:503
  34.9 0.0 copy-done.1
  34.9 0.0 copy-done.2
  34.9 0.0 copy-done.3
  34.9 0.0 copy-done.14
  34.9 2.6 %expert.1 = bf16[32,4,640]{2,1,0:T(4,128)(2,1)S(1)} custom-call(bf16[32,4,640]{2,1,0:T(4,128)(2,1)S(1)} %all_to_all.10.arrived_ref, f32[1,2048]{1,0:T(1,128)S(1)} %bitcast.25, bf16[2048,1024]{1,0:T(8,128)(2,1)S(1)} %bitcast.17, bf16[2048,1024]{1,0:T(8,128)(2,1)S(1)} %bitcast.18, bf16[1024,2048]{1,0:T(8,128)(2,1)S(1)} %bitcast.19), custom_call_target="tpu_custom_call" | custom-call | tf_op jit(solution)/shard_map/expert/pallas_call | solution.py:505
  37.5 10.7 %all_to_all.11.returned_ref = bf16[32,4,640]{2,1,0:T(4,128)(2,1)S(1)} all-to-all(bf16[32,4,640]{2,1,0:T(4,128)(2,1)S(1)} %expert.1), channel_id=1, replica_groups=mesh['ep'=8,'tp'=4] {'ep','tp'}, dimensions={0} | all-to-all | bytes 327680 | tf_op jit(solution)/shard_map/all_to_all | solution.py:503
  48.2 0.9 %combine.1 = bf16[48,512]{1,0:T(8,128)(2,1)} custom-call(bf16[32,4,640]{2,1,0:T(4,128)(2,1)S(1)} %all_to_all.11.returned_ref, bf16[48,512]{1,0:T(8,128)(2,1)S(1)} %get-tuple-element.20.residual_ref, bf16[48,160]{1,0:T(8,128)(2,1)S(1)} %get-tuple-element.21.high_ref, bf16[48,160]{1,0:T(8,128)(2,1)S(1)} %get-tuple-element.22.low_ref), custom_call_target="tpu_custom_call" | custom-call | tf_op jit(solution)/shard_map/combine/pallas_call | solution.py:520
  (4 shorter events, 0.0 us)
Async XLA Ops:
  0.0 9.7 %copy-start.6 = (bf16[512,2048]{1,0:T(8,128)(2,1)S(1)}, bf16[512,2048]{1,0:T(8,128)(2,1)}, u32[]{:S(2)}) copy-start(bf16[512,2048]{1,0:T(8,128)(2,1)} %out_w.1) | copy-start | bytes 6291460
  0.0 9.7 %copy-start.18 = (f32[512]{0:T(512)S(1)}, f32[512]{0:T(512)}, u32[]{:S(2)}) copy-start(f32[512]{0:T(512)} %param.42) | copy-start | bytes 6148
  0.0 9.7 %copy-start.12 = (bf16[48,3,256]{2,0,1:T(8,128)(2,1)S(1)}, bf16[48,3,256]{2,0,1:T(8,128)(2,1)}, u32[]{:S(2)}) copy-start(bf16[48,3,256]{2,0,1:T(8,128)(2,1)} %param.40) | copy-start | bytes 221188
  0.0 9.7 %copy-start.11 = (bf16[48,3,256]{2,0,1:T(8,128)(2,1)S(1)}, bf16[48,3,256]{2,0,1:T(8,128)(2,1)}, u32[]{:S(2)}) copy-start(bf16[48,3,256]{2,0,1:T(8,128)(2,1)} %param.39) | copy-start | bytes 221188
  0.0 9.7 %copy-start.9 = (bf16[48,3,512]{2,0,1:T(8,128)(2,1)S(1)}, bf16[48,3,512]{2,0,1:T(8,128)(2,1)}, u32[]{:S(2)}) copy-start(bf16[48,3,512]{2,0,1:T(8,128)(2,1)} %param.38) | copy-start | bytes 442372
  0.0 9.7 %copy-start.17 = (bf16[4,256]{1,0:T(4,128)(2,1)S(1)}, bf16[4,256]{1,0:T(4,128)(2,1)}, u32[]{:S(2)}) copy-start(bf16[4,256]{1,0:T(4,128)(2,1)} %tap_c_ref.1) | copy-start | bytes 6148
  0.0 9.7 %copy-start.16 = (bf16[4,256]{1,0:T(4,128)(2,1)S(1)}, bf16[4,256]{1,0:T(4,128)(2,1)}, u32[]{:S(2)}) copy-start(bf16[4,256]{1,0:T(4,128)(2,1)} %tap_b_ref.1) | copy-start | bytes 6148
  0.0 9.7 %copy-start.15 = (bf16[4,512]{1,0:T(4,128)(2,1)S(1)}, bf16[4,512]{1,0:T(4,128)(2,1)}, u32[]{:S(2)}) copy-start(bf16[4,512]{1,0:T(4,128)(2,1)} %tap_x_ref.1) | copy-start | bytes 12292
  0.0 9.7 %copy-start.21 = (f32[32]{0:T(128)S(1)}, f32[32]{0:T(128)}, u32[]{:S(2)}) copy-start(f32[32]{0:T(128)} %param.34) | copy-start | bytes 388
  0.1 9.7 %copy-start.20 = (f32[32]{0:T(128)S(1)}, f32[32]{0:T(128)}, u32[]{:S(2)}) copy-start(f32[32]{0:T(128)} %param.33) | copy-start | bytes 388
  0.1 9.7 %copy-start.19 = (f32[32]{0:T(128)S(1)}, f32[32]{0:T(128)}, u32[]{:S(2)}) copy-start(f32[32]{0:T(128)} %param.32) | copy-start | bytes 388
  0.1 9.7 %copy-start.10 = (bf16[2048,32]{0,1:T(8,128)(2,1)S(1)}, bf16[2048,32]{0,1:T(8,128)(2,1)}, u32[]{:S(2)}) copy-start(bf16[2048,32]{0,1:T(8,128)(2,1)} %param.31) | copy-start | bytes 393220
  0.1 9.7 %copy-start.8 = (bf16[2048,256]{1,0:T(8,128)(2,1)S(1)}, bf16[2048,256]{1,0:T(8,128)(2,1)}, u32[]{:S(2)}) copy-start(bf16[2048,256]{1,0:T(8,128)(2,1)} %query_w.1) | copy-start | bytes 3145732
  0.1 9.7 %copy-start.7 = (bf16[2048,256]{1,0:T(8,128)(2,1)S(1)}, bf16[2048,256]{1,0:T(8,128)(2,1)}, u32[]{:S(2)}) copy-start(bf16[2048,256]{1,0:T(8,128)(2,1)} %key_w.1) | copy-start | bytes 3145732
  0.1 9.7 %copy-start.5 = (bf16[2048,512]{1,0:T(8,128)(2,1)S(1)}, bf16[2048,512]{1,0:T(8,128)(2,1)}, u32[]{:S(2)}) copy-start(bf16[2048,512]{1,0:T(8,128)(2,1)} %value_w.1) | copy-start | bytes 6291460
  0.1 9.7 %copy-start.4 = (bf16[2048,512]{1,0:T(8,128)(2,1)S(1)}, bf16[2048,512]{1,0:T(8,128)(2,1)}, u32[]{:S(2)}) copy-start(bf16[2048,512]{1,0:T(8,128)(2,1)} %gate_w.1) | copy-start | bytes 6291460
  0.1 9.7 %copy-start.13 = (f32[2048]{0:T(1024)S(1)}, f32[2048]{0:T(1024)}, u32[]{:S(2)}) copy-start(f32[2048]{0:T(1024)} %param.26) | copy-start | bytes 24580
  0.1 9.7 %copy-start = (f32[48,8,64,128]{3,2,1,0:T(8,128)S(1)}, f32[48,8,64,128]{3,2,1,0:T(8,128)}, u32[]{:S(2)}) copy-start(f32[48,8,64,128]{3,2,1,0:T(8,128)} %param.41) | copy-start | bytes 37748740
  1.1 6.1 %collective-permute-start.2 = (bf16[48,512]{1,0:T(8,128)(2,1)S(1)}, bf16[48,512]{1,0:T(8,128)(2,1)S(1)}, u32[]{:S(2)}, u32[]{:S(2)}) collective-permute-start(bf16[48,512]{1,0:T(8,128)(2,1)S(1)} %entry.1.own_ref), channel_id=1, source_target_pairs={{0,3},{1,2},{2,1},{3,0},{4,7},{5,6},{6,5},{7,4},{8,11},{9,10},{10,... | collective-permute-start | bytes 147464 | tf_op jit(solution)/shard_map/ppermute | solution.py:430
  5.1 4.1 %collective-permute-start.1 = (bf16[48,512]{1,0:T(8,128)(2,1)S(1)}, bf16[48,512]{1,0:T(8,128)(2,1)S(1)}, u32[]{:S(2)}, u32[]{:S(2)}) collective-permute-start(bf16[48,512]{1,0:T(8,128)(2,1)S(1)} %entry.1.own_ref), channel_id=1, source_target_pairs={{0,2},{1,3},{2,0},{3,1},{4,6},{5,7},{6,4},{7,5},{8,10},{9,11},{10,... | collective-permute-start | bytes 147464 | tf_op jit(solution)/shard_map/ppermute | solution.py:430
  5.6 4.1 %collective-permute-start = (bf16[48,512]{1,0:T(8,128)(2,1)S(1)}, bf16[48,512]{1,0:T(8,128)(2,1)S(1)}, u32[]{:S(2)}, u32[]{:S(2)}) collective-permute-start(bf16[48,512]{1,0:T(8,128)(2,1)S(1)} %entry.1.own_ref), channel_id=1, source_target_pairs={{0,1},{1,0},{2,3},{3,2},{4,5},{5,4},{6,7},{7,6},{8,9},{9,8},{10,11... | collective-permute-start | bytes 147464 | tf_op jit(solution)/shard_map/ppermute | solution.py:430
  9.9 7.7 %copy-start.22 = (s32[48,2]{0,1:T(2,128)S(1)}, s32[48,2]{0,1:T(2,128)}, u32[]{:S(2)}) copy-start(s32[48,2]{0,1:T(2,128)} %param.45) | copy-start | bytes 1156
  9.9 7.7 %copy-start.23 = (f32[48,2]{0,1:T(2,128)S(1)}, f32[48,2]{0,1:T(2,128)}, u32[]{:S(2)}) copy-start(f32[48,2]{0,1:T(2,128)} %param.46) | copy-start | bytes 1156
  14.0 4.5 %collective-permute-start.3 = (bf16[48,512]{1,0:T(8,128)(2,1)S(1)}, bf16[48,512]{1,0:T(8,128)(2,1)S(1)}, u32[]{:S(2)}, u32[]{:S(2)}) collective-permute-start(bf16[48,512]{1,0:T(8,128)(2,1)S(1)} %get-tuple-element.15), channel_id=1, source_target_pairs={{0,1},{1,0},{2,3},{3,2},{4,5},{5,4},{6,7},{7,6},{8,9},{9,8},{10,11... | collective-permute-start | bytes 147464 | tf_op jit(solution)/shard_map/ppermute | solution.py:430
  14.4 4.1 %collective-permute-start.4 = (bf16[48,512]{1,0:T(8,128)(2,1)S(1)}, bf16[48,512]{1,0:T(8,128)(2,1)S(1)}, u32[]{:S(2)}, u32[]{:S(2)}) collective-permute-start(bf16[48,512]{1,0:T(8,128)(2,1)S(1)} %get-tuple-element.16), channel_id=1, source_target_pairs={{0,2},{1,3},{2,0},{3,1},{4,6},{5,7},{6,4},{7,5},{8,10},{9,11},{10,... | collective-permute-start | bytes 147464 | tf_op jit(solution)/shard_map/ppermute | solution.py:430
  16.1 5.0 %collective-permute-start.5 = (bf16[48,512]{1,0:T(8,128)(2,1)S(1)}, bf16[48,512]{1,0:T(8,128)(2,1)S(1)}, u32[]{:S(2)}, u32[]{:S(2)}) collective-permute-start(bf16[48,512]{1,0:T(8,128)(2,1)S(1)} %get-tuple-element.17), channel_id=1, source_target_pairs={{0,3},{1,2},{2,1},{3,0},{4,7},{5,6},{6,5},{7,4},{8,11},{9,10},{10,... | collective-permute-start | bytes 147464 | tf_op jit(solution)/shard_map/ppermute | solution.py:430
  17.6 17.3 %copy-start.1 = (bf16[1,2048,1024]{2,1,0:T(8,128)(2,1)S(1)}, bf16[1,2048,1024]{2,1,0:T(8,128)(2,1)}, u32[]{:S(2)}) copy-start(bf16[1,2048,1024]{2,1,0:T(8,128)(2,1)} %param.47) | copy-start | bytes 12582916
  17.6 17.3 %copy-start.2 = (bf16[1,2048,1024]{2,1,0:T(8,128)(2,1)S(1)}, bf16[1,2048,1024]{2,1,0:T(8,128)(2,1)}, u32[]{:S(2)}) copy-start(bf16[1,2048,1024]{2,1,0:T(8,128)(2,1)} %param.48) | copy-start | bytes 12582916
  17.6 17.3 %copy-start.3 = (bf16[1,1024,2048]{2,1,0:T(8,128)(2,1)S(1)}, bf16[1,1024,2048]{2,1,0:T(8,128)(2,1)}, u32[]{:S(2)}) copy-start(bf16[1,1024,2048]{2,1,0:T(8,128)(2,1)} %param.49) | copy-start | bytes 12582916
  17.6 17.3 %copy-start.14 = (f32[2048]{0:T(1024)S(1)}, f32[2048]{0:T(1024)}, u32[]{:S(2)}) copy-start(f32[2048]{0:T(1024)} %param.44) | copy-start | bytes 24580

commit v4 on v3

--- a/solution.py
+++ b/solution.py
@@ -153,26 +153,20 @@
 
 ROW_TILE = 8
 LANES = 128
+VECTOR_SEQS = 16
 
 
 def dot_bf16(left, right):
     return lax.dot_general(left, right, (((1,), (0,)), ((), ())), preferred_element_type=jnp.float32)
 
 
-def dot_nt(left, right, precision=None):
-    return lax.dot_general(
-        left, right, (((1,), (1,)), ((), ())), precision=precision, preferred_element_type=jnp.float32
-    )
-
-
-def dot_exact(left, right):
-    return lax.dot_general(
-        left,
-        right,
-        (((1,), (0,)), ((), ())),
-        precision=lax.Precision.HIGHEST,
-        preferred_element_type=jnp.float32,
-    )
+def dot_nt(left, right):
+    return lax.dot_general(left, right, (((1,), (1,)), ((), ())), preferred_element_type=jnp.float32)
+
+
+def halves(array):
+    high = array.astype(jnp.bfloat16)
+    return high, (array - high.astype(jnp.float32)).astype(jnp.bfloat16)
 
 
 def silu(value):
@@ -212,6 +206,7 @@
     part_refs,
     y_ref,
     row_ref,
+    query_ref,
 ):
     tp_index = lax.axis_index("tp")
     seqs, width = y_ref.shape
@@ -228,34 +223,57 @@
     normed = (rows * scale * gain_ref[...]).astype(jnp.bfloat16)
     step_size = jax.nn.softplus(dot_nt(normed, step_w_ref[...]) + bias_ref[...])
     decay = jnp.exp(-step_size * jnp.exp(rate_ref[...]))
-    keys = conv_rows(win_b_ref, columns, dot_bf16(normed, key_w[:, columns]), tap_b_ref)
-    queries = conv_rows(win_c_ref, columns, dot_bf16(normed, query_w[:, columns]), tap_c_ref)
+    key_row = dot_bf16(normed, key_w[:, columns])
+    query_row = dot_bf16(normed, query_w[:, columns])
+    value_row = dot_bf16(normed, value_w[...])
+    gate_z = dot_bf16(normed, gate_w[...])
+    keys = conv_rows(win_b_ref, columns, key_row, tap_b_ref)
+    queries = conv_rows(win_c_ref, columns, query_row, tap_c_ref)
     overlap = jnp.sum(keys * queries, axis=-1, keepdims=True)
-    query_hi = queries.astype(jnp.bfloat16)
-    query_lo = (queries - query_hi.astype(jnp.float32)).astype(jnp.bfloat16)
+    query_hi, query_lo = halves(queries)
     row_of = lax.broadcasted_iota(jnp.int32, (ROW_TILE, width), 0)
-    for b in range(blocks):
-        lines = slice(b * ROW_TILE, (b + 1) * ROW_TILE)
-        both = jnp.concatenate([query_hi[lines], query_lo[lines]], axis=0)
-        total = jnp.zeros((ROW_TILE, width), jnp.float32)
-        for i in range(ROW_TILE):
-            found = dot_nt(both, state[b * ROW_TILE + i].astype(jnp.bfloat16))
-            total = jnp.where(row_of == i, found[:ROW_TILE] + found[ROW_TILE:], total)
-        y_ref[lines] = total
+    lane = lax.broadcasted_iota(jnp.int32, (LANES, LANES), 1)
+    query_ref[...] = queries
+    first_block = VECTOR_SEQS // ROW_TILE
+    for b in range(max(blocks - first_block, width // LANES)):
+        if b < width // LANES:
+            span = slice(b * LANES, (b + 1) * LANES)
+            turned = jnp.zeros((LANES, LANES), jnp.float32)
+            for i in range(VECTOR_SEQS):
+                summed = jnp.sum(state[i, span] * query_ref[i : i + 1], axis=-1, keepdims=True)
+                turned = jnp.where(lane == i, summed, turned)
+            y_ref[:VECTOR_SEQS, span] = turned.T[:VECTOR_SEQS]
+        if first_block + b < blocks:
+            start = (first_block + b) * ROW_TILE
+            lines = slice(start, start + ROW_TILE)
+            both = jnp.concatenate([query_hi[lines], query_lo[lines]], axis=0)
+            total = jnp.zeros((ROW_TILE, width), jnp.float32)
+            for i in range(ROW_TILE):
+                found = dot_nt(both, state[start + i].astype(jnp.bfloat16))
+                total = jnp.where(row_of == i, found[:ROW_TILE] + found[ROW_TILE:], total)
+            y_ref[lines] = total
     spread = (
-        lax.broadcasted_iota(jnp.int32, (HEADS, width), 0)
-        == first_head + lax.broadcasted_iota(jnp.int32, (HEADS, width), 1) // HEAD_DIM
-    ).astype(jnp.float32)
-    values = conv_rows(win_x_ref, slice(None), dot_bf16(normed, value_w[...]), tap_x_ref)
-    gate_z = dot_bf16(normed, gate_w[...])
-    read_out = (
-        dot_exact(decay, spread) * y_ref[...]
-        + (dot_exact(step_size, spread) * overlap + dot_exact(skip_ref[...], spread)) * values
-    )
+        lax.broadcasted_iota(jnp.int32, (2 * HEADS, width), 0) % HEADS
+        == first_head + lax.broadcasted_iota(jnp.int32, (2 * HEADS, width), 1) // HEAD_DIM
+    ).astype(jnp.bfloat16)
+    per_head = jnp.concatenate(
+        [decay, step_size, jnp.broadcast_to(skip_ref[...], (ROW_TILE, HEADS))], axis=0
+    )
+    wide = dot_bf16(jnp.concatenate(halves(per_head), axis=1), spread)
+    values = conv_rows(win_x_ref, slice(None), value_row, tap_x_ref)
+    read_out = wide[:seqs] * y_ref[...] + (wide[seqs : 2 * seqs] * overlap + wide[2 * seqs : 2 * seqs + 1]) * values
     gated = read_out * silu(gate_z)
-    mean_sq = dot_nt(gated * gated, spread, lax.Precision.HIGHEST) * (1.0 / HEAD_DIM)
-    scale_heads = dot_exact(lax.rsqrt(mean_sq + norm_epsilon), spread)
-    mixed = (gated * scale_heads * head_gain_ref[...]).astype(jnp.bfloat16)
+    same_head = (
+        lax.broadcasted_iota(jnp.int32, (LANES, LANES), 0) // HEAD_DIM
+        == lax.broadcasted_iota(jnp.int32, (LANES, LANES), 1) // HEAD_DIM
+    ).astype(jnp.bfloat16)
+    scaled = []
+    for j in range(0, width, LANES):
+        block = gated[:, j : j + LANES]
+        sums = dot_bf16(jnp.concatenate(halves(block * block), axis=0), same_head)
+        mean_sq = (sums[:seqs] + sums[seqs:]) * (1.0 / HEAD_DIM)
+        scaled.append(block * lax.rsqrt(mean_sq + norm_epsilon) * head_gain_ref[:, j : j + LANES])
+    mixed = jnp.concatenate(scaled, axis=1).astype(jnp.bfloat16)
     for k, part_ref in enumerate(part_refs):
         span = pl.ds(pl.multiple_of((tp_index ^ k) * own_width, own_width), own_width)
         part_ref[...] = dot_bf16(mixed, out_w[:, span]).astype(part_ref.dtype)
@@ -264,7 +282,8 @@
 def slots_of(ids_ref, experts, lines):
     seqs = ids_ref.shape[1]
     line = lax.broadcasted_iota(jnp.int32, (lines, seqs), 0)
-    expert = line % experts
+    sets = lax.axis_size("ep")
+    expert = line % sets * EXP_IN + line % experts // sets
     first = ids_ref[0:1, :] == expert
     second = ids_ref[1:2, :] == expert
     hit = jnp.logical_or(first, second)
@@ -276,10 +295,15 @@
     return jnp.logical_and(hit, rank == place), first
 
 
-def entry_body(own_hbm, own_ref, sem):
-    copy = pltpu.make_async_copy(own_hbm, own_ref, sem)
-    copy.start()
-    copy.wait()
+def entry_body(own_hbm, own_ref, sems):
+    copies = []
+    for i in range(sems.shape[0]):
+        span = pl.ds(i * ROW_TILE, ROW_TILE)
+        copies.append(pltpu.make_async_copy(own_hbm.at[span], own_ref.at[span], sems.at[i]))
+    for copy in copies:
+        copy.start()
+    for copy in copies:
+        copy.wait()
 
 
 def route_body(ids_ref, weight_ref, chosen_ref, high_ref, low_ref):
@@ -289,9 +313,7 @@
     weights = weight_ref[...]
     share = weights / jnp.sum(weights, axis=0, keepdims=True)
     picked = jnp.where(chosen, jnp.where(first, share[0:1, :], share[1:2, :]), 0.0).T
-    high = picked.astype(jnp.bfloat16)
-    high_ref[...] = high
-    low_ref[...] = (picked - high.astype(jnp.float32)).astype(jnp.bfloat16)
+    high_ref[...], low_ref[...] = halves(picked)
 
 
 def write_blocks(line_ref, moved_ref):
@@ -338,7 +360,7 @@
         (
             slice(k * ep_count, (k + 1) * ep_count),
             slice(part * own_width + j * LANES, part * own_width + (j + 1) * LANES),
-            pl.ds(part * blocks + j, ep_count, stride=tp_count * blocks),
+            pl.ds(part * ep_count * blocks + j, ep_count, stride=blocks),
             k,
         )
         for k in range(width // LANES)
@@ -434,7 +456,7 @@
         out_shape=pltpu.VMEM((seqs, own_width), bf16),
         in_specs=[IN_HBM],
         out_specs=IN_VMEM,
-        scratch_shapes=[pltpu.SemaphoreType.DMA],
+        scratch_shapes=[pltpu.SemaphoreType.DMA((seqs // ROW_TILE,))],
         compiler_params=grant(4),
         cost_estimate=pl.CostEstimate(flops=2 * 10**10, bytes_accessed=2**25, transcendentals=0),
         name="entry",
@@ -463,6 +485,7 @@
         scratch_shapes=[
             pltpu.VMEM((seqs, width), f32),
             pltpu.VMEM((seqs, model_width), bf16),
+            pltpu.VMEM((seqs, STATE), f32),
         ],
         compiler_params=grant(4),
         name="mixer",
@@ -500,7 +523,7 @@
     )(own, shares, chosen)
 
     def exchange(sent):
-        return lax.all_to_all(sent, ("ep", "tp"), split_axis=0, concat_axis=0, tiled=True)
+        return lax.all_to_all(sent, ("tp", "ep"), split_axis=0, concat_axis=0, tiled=True)
 
     result = pl.pallas_call(
         expert_body,

time: 49.3 us -> 47.6 us (0.966)
  Pallas kernels: 9.01 us -> 7.76 us
    pallas_call x1, Pallas kernels: 4.12 us -> 3.05 us  [local_fast(): pl.pallas_call(mixer_body, out_shape=((pltpu.VMEM((seqs, own_width), f32)...]
  transfers between devices with their start and end apart: 6 -> 6, of which waited for: 5 -> 6; matrix products, arithmetic and copies ran while one was open for 0% -> 0% of each run, Pallas kernels for 0% -> 0%
where the time goes in v4:
time: 47.6 us; the launch traced here: 47.4 us
  blocking collectives  23.8 us (50%)
  starting transfers between devices  8.2 us (17%)
  Pallas kernels  7.76 us (16%)
  waiting for transfers between devices  7.25 us (15%)
    all_to_all x2, blocking collectives, exchange(): lax.all_to_all(sent, ('tp', 'ep'), split_axis=0, concat_axis=0, tiled=True)  23.8 us
    ppermute x6, starting transfers between devices, shift(): return lax.ppermute(array, 'tp', [(i, i ^ k) for i in range(tp_count)])  8.2 us
    ppermute x6, waiting for transfers between devices, shift(): return lax.ppermute(array, 'tp', [(i, i ^ k) for i in range(tp_count)])  7.25 us
    pallas_call x1, Pallas kernels, local_fast(): pl.pallas_call(mixer_body, out_shape=((pltpu.VMEM((seqs, own_width), f32)...  3.05 us
    pallas_call x1, Pallas kernels, local_fast(): pl.pallas_call(expert_body, out_shape=pltpu.VMEM(moved_shape, bf16), in_s...  2.45 us
  transfers between devices with their start and end apart: 6, of which 6 were waited for; matrix products, arithmetic and copies ran while one was open for 0% of the time, Pallas kernels for 0%

profile of v4, /device:TPU:0, one launch (start us, length us, event | category | flops | bytes accessed | tf_op | source)
XLA Modules:
  0.0 47.4 jit_solution(86945211277636008)
XLA Ops:
  0.0 0.0 copy-start.18
  0.0 0.0 copy-start.12
  0.0 0.0 copy-start.11
  0.0 0.0 copy-start.17
  0.0 0.0 copy-start.16
  0.0 0.0 copy-start.15
  0.0 0.0 copy-start.21
  0.1 0.0 copy-start.20
  0.1 0.0 copy-start.19
  0.1 0.0 copy-start.10
  0.1 0.0 copy-start.8
  0.1 0.0 copy-start.7
  0.1 0.0 copy-start.5
  0.1 0.0 copy-start.4
  0.1 0.0 copy-start.13
  0.1 0.0 copy-start
  0.1 0.9 %entry.1.own_ref = bf16[48,512]{1,0:T(8,128)(2,1)S(1)} custom-call(bf16[48,512]{1,0:T(8,128)(2,1)} %own_hbm.1), custom_call_target="tpu_custom_call" | custom-call | flops 20000000000 | bytes 33554432 | tf_op jit(solution)/shard_map/entry/pallas_call | solution.py:454
  1.1 4.0 %collective-permute-start.2 = (bf16[48,512]{1,0:T(8,128)(2,1)S(1)}, bf16[48,512]{1,0:T(8,128)(2,1)S(1)}, u32[]{:S(2)}, u32[]{:S(2)}) collective-permute-start(bf16[48,512]{1,0:T(8,128)(2,1)S(1)} %entry.1.own_ref), channel_id=1, source_target_pairs={{0,3},{1,2},{2,1},{3,0},{4,7},{5,6},{6,5},{7,4},{8,11},{9,10},{10,... | collective-permute-start | bytes 147464 | tf_op jit(solution)/shard_map/ppermute | solution.py:452
  5.1 0.5 %collective-permute-start.1 = (bf16[48,512]{1,0:T(8,128)(2,1)S(1)}, bf16[48,512]{1,0:T(8,128)(2,1)S(1)}, u32[]{:S(2)}, u32[]{:S(2)}) collective-permute-start(bf16[48,512]{1,0:T(8,128)(2,1)S(1)} %entry.1.own_ref), channel_id=1, source_target_pairs={{0,2},{1,3},{2,0},{3,1},{4,6},{5,7},{6,4},{7,5},{8,10},{9,11},{10,... | collective-permute-start | bytes 147464 | tf_op jit(solution)/shard_map/ppermute | solution.py:452
  5.6 0.1 collective-permute-start
  5.7 1.4 %collective-permute-done.2.piece_refs_2_ = bf16[48,512]{1,0:T(8,128)(2,1)S(1)} collective-permute-done((bf16[48,512]{1,0:T(8,128)(2,1)S(1)}, bf16[48,512]{1,0:T(8,128)(2,1)S(1)}, u32[]{:S(2)}, u32[]{:S(2)}) %collective-permute-start.2) | collective-permute-done | bytes 49184 | tf_op jit(solution)/shard_map/ppermute | solution.py:452
  7.1 2.0 %collective-permute-done.1.piece_refs_1_ = bf16[48,512]{1,0:T(8,128)(2,1)S(1)} collective-permute-done((bf16[48,512]{1,0:T(8,128)(2,1)S(1)}, bf16[48,512]{1,0:T(8,128)(2,1)S(1)}, u32[]{:S(2)}, u32[]{:S(2)}) %collective-permute-start.1) | collective-permute-done | bytes 49184 | tf_op jit(solution)/shard_map/ppermute | solution.py:452
  9.2 0.5 %collective-permute-done.piece_refs_0_ = bf16[48,512]{1,0:T(8,128)(2,1)S(1)} collective-permute-done((bf16[48,512]{1,0:T(8,128)(2,1)S(1)}, bf16[48,512]{1,0:T(8,128)(2,1)S(1)}, u32[]{:S(2)}, u32[]{:S(2)}) %collective-permute-start) | collective-permute-done | bytes 49184 | tf_op jit(solution)/shard_map/ppermute | solution.py:452
  9.7 0.0 copy-done.6
  9.7 0.0 copy-done.18
  9.7 0.0 copy-done.12
  9.7 0.0 copy-done.11
  9.7 0.0 copy-done.9
  9.7 0.0 copy-done.17
  9.7 0.0 copy-done.16
  9.7 0.0 copy-done.15
  9.7 0.0 copy-done.21
  9.7 0.0 copy-done.20
  9.7 0.0 copy-done.19
  9.8 0.0 copy-done.10
  9.8 0.0 copy-done.8
  9.8 0.0 copy-done.7
  9.8 0.0 copy-done.5
  9.8 0.0 copy-done.4
  9.8 0.0 copy-done.13
  9.8 0.0 copy-done
  9.8 0.0 copy-start.22
  9.8 0.0 copy-start.23
  9.8 3.0 %mixer.1 = (f32[48,512]{1,0:T(8,128)S(1)}, bf16[48,512]{1,0:T(8,128)(2,1)S(1)}, bf16[48,512]{1,0:T(8,128)(2,1)S(1)}, bf16[48,512]{1,0:T(8,128)(2,1)S(1)}) custom-call(bf16[48,512]{1,0:T(8,128)(2,1)S(1)} %entry.1.own_ref, bf16[48,512]{1,0:T(8,128)(2,1)S(1)} %collective-permute-done.piece_refs_0_, bf16[48,512]{1,0:T(8,128)(2,1)S(1)} %collective-permute-done.1.piece_refs_1_, ...), custom_call_target="tpu_custom_call" | custom-call | tf_op jit(solution)/shard_map/mixer/pallas_call | solution.py:478
  12.9 0.5 collective-permute-start.3
  13.4 1.7 %collective-permute-start.4 = (bf16[48,512]{1,0:T(8,128)(2,1)S(1)}, bf16[48,512]{1,0:T(8,128)(2,1)S(1)}, u32[]{:S(2)}, u32[]{:S(2)}) collective-permute-start(bf16[48,512]{1,0:T(8,128)(2,1)S(1)} %get-tuple-element.16), channel_id=1, source_target_pairs={{0,2},{1,3},{2,0},{3,1},{4,6},{5,7},{6,4},{7,5},{8,10},{9,11},{10,... | collective-permute-start | bytes 147464 | tf_op jit(solution)/shard_map/ppermute | solution.py:452
  15.0 1.4 %collective-permute-start.5 = (bf16[48,512]{1,0:T(8,128)(2,1)S(1)}, bf16[48,512]{1,0:T(8,128)(2,1)S(1)}, u32[]{:S(2)}, u32[]{:S(2)}) collective-permute-start(bf16[48,512]{1,0:T(8,128)(2,1)S(1)} %get-tuple-element.17), channel_id=1, source_target_pairs={{0,3},{1,2},{2,1},{3,0},{4,7},{5,6},{6,5},{7,4},{8,11},{9,10},{10,... | collective-permute-start | bytes 147464 | tf_op jit(solution)/shard_map/ppermute | solution.py:452
  16.5 0.0 copy-done.22
  16.5 0.0 copy-done.23
  16.5 0.0 copy-start.3
  16.5 0.0 copy-start.14
  16.5 0.2 route.1
  16.7 0.7 %collective-permute-done.3.part_refs_1_ = bf16[48,512]{1,0:T(8,128)(2,1)S(1)} collective-permute-done((bf16[48,512]{1,0:T(8,128)(2,1)S(1)}, bf16[48,512]{1,0:T(8,128)(2,1)S(1)}, u32[]{:S(2)}, u32[]{:S(2)}) %collective-permute-start.3) | collective-permute-done | bytes 49184 | tf_op jit(solution)/shard_map/ppermute | solution.py:452
  17.4 0.1 collective-permute-done.4.part_refs_2_
  17.5 2.6 %collective-permute-done.5.part_refs_3_ = bf16[48,512]{1,0:T(8,128)(2,1)S(1)} collective-permute-done((bf16[48,512]{1,0:T(8,128)(2,1)S(1)}, bf16[48,512]{1,0:T(8,128)(2,1)S(1)}, u32[]{:S(2)}, u32[]{:S(2)}) %collective-permute-start.5) | collective-permute-done | bytes 49184 | tf_op jit(solution)/shard_map/ppermute | solution.py:452
  20.0 0.2 pack.1
  20.3 13.2 %all_to_all.10.arrived_ref = bf16[32,4,640]{2,1,0:T(4,128)(2,1)S(1)} all-to-all(bf16[32,4,640]{2,1,0:T(4,128)(2,1)S(1)} %get-tuple-element.19), channel_id=1, replica_groups=mesh['ep'=8,'tp'=4] {'tp','ep'}, dimensions={0} | all-to-all | bytes 327680 | tf_op jit(solution)/shard_map/all_to_all | solution.py:526
  33.5 0.0 copy-done.1
  33.5 0.0 copy-done.2
  33.5 0.0 copy-done.3
  33.5 0.0 copy-done.14
  33.5 2.4 %expert.1 = bf16[32,4,640]{2,1,0:T(4,128)(2,1)S(1)} custom-call(bf16[32,4,640]{2,1,0:T(4,128)(2,1)S(1)} %all_to_all.10.arrived_ref, f32[1,2048]{1,0:T(1,128)S(1)} %bitcast.25, bf16[2048,1024]{1,0:T(8,128)(2,1)S(1)} %bitcast.17, bf16[2048,1024]{1,0:T(8,128)(2,1)S(1)} %bitcast.18, bf16[1024,2048]{1,0:T(8,128)(2,1)S(1)} %bitcast.19), custom_call_target="tpu_custom_call" | custom-call | tf_op jit(solution)/shard_map/expert/pallas_call | solution.py:528
  36.0 10.5 %all_to_all.11.returned_ref = bf16[32,4,640]{2,1,0:T(4,128)(2,1)S(1)} all-to-all(bf16[32,4,640]{2,1,0:T(4,128)(2,1)S(1)} %expert.1), channel_id=1, replica_groups=mesh['ep'=8,'tp'=4] {'tp','ep'}, dimensions={0} | all-to-all | bytes 327680 | tf_op jit(solution)/shard_map/all_to_all | solution.py:526
  46.5 0.9 %combine.1 = bf16[48,512]{1,0:T(8,128)(2,1)} custom-call(bf16[32,4,640]{2,1,0:T(4,128)(2,1)S(1)} %all_to_all.11.returned_ref, bf16[48,512]{1,0:T(8,128)(2,1)S(1)} %get-tuple-element.20.residual_ref, bf16[48,160]{1,0:T(8,128)(2,1)S(1)} %get-tuple-element.21.high_ref, bf16[48,160]{1,0:T(8,128)(2,1)S(1)} %get-tuple-element.22.low_ref), custom_call_target="tpu_custom_call" | custom-call | tf_op jit(solution)/shard_map/combine/pallas_call | solution.py:543
  (4 shorter events, 0.0 us)
Async XLA Ops:
  0.0 9.7 %copy-start.6 = (bf16[512,2048]{1,0:T(8,128)(2,1)S(1)}, bf16[512,2048]{1,0:T(8,128)(2,1)}, u32[]{:S(2)}) copy-start(bf16[512,2048]{1,0:T(8,128)(2,1)} %out_w.1) | copy-start | bytes 6291460
  0.0 9.7 %copy-start.18 = (f32[512]{0:T(512)S(1)}, f32[512]{0:T(512)}, u32[]{:S(2)}) copy-start(f32[512]{0:T(512)} %param.42) | copy-start | bytes 6148
  0.0 9.7 %copy-start.12 = (bf16[48,3,256]{2,0,1:T(8,128)(2,1)S(1)}, bf16[48,3,256]{2,0,1:T(8,128)(2,1)}, u32[]{:S(2)}) copy-start(bf16[48,3,256]{2,0,1:T(8,128)(2,1)} %param.40) | copy-start | bytes 221188
  0.0 9.7 %copy-start.11 = (bf16[48,3,256]{2,0,1:T(8,128)(2,1)S(1)}, bf16[48,3,256]{2,0,1:T(8,128)(2,1)}, u32[]{:S(2)}) copy-start(bf16[48,3,256]{2,0,1:T(8,128)(2,1)} %param.39) | copy-start | bytes 221188
  0.0 9.7 %copy-start.9 = (bf16[48,3,512]{2,0,1:T(8,128)(2,1)S(1)}, bf16[48,3,512]{2,0,1:T(8,128)(2,1)}, u32[]{:S(2)}) copy-start(bf16[48,3,512]{2,0,1:T(8,128)(2,1)} %param.38) | copy-start | bytes 442372
  0.0 9.7 %copy-start.17 = (bf16[4,256]{1,0:T(4,128)(2,1)S(1)}, bf16[4,256]{1,0:T(4,128)(2,1)}, u32[]{:S(2)}) copy-start(bf16[4,256]{1,0:T(4,128)(2,1)} %tap_c_ref.1) | copy-start | bytes 6148
  0.0 9.7 %copy-start.16 = (bf16[4,256]{1,0:T(4,128)(2,1)S(1)}, bf16[4,256]{1,0:T(4,128)(2,1)}, u32[]{:S(2)}) copy-start(bf16[4,256]{1,0:T(4,128)(2,1)} %tap_b_ref.1) | copy-start | bytes 6148
  0.0 9.7 %copy-start.15 = (bf16[4,512]{1,0:T(4,128)(2,1)S(1)}, bf16[4,512]{1,0:T(4,128)(2,1)}, u32[]{:S(2)}) copy-start(bf16[4,512]{1,0:T(4,128)(2,1)} %tap_x_ref.1) | copy-start | bytes 12292
  0.0 9.7 %copy-start.21 = (f32[32]{0:T(128)S(1)}, f32[32]{0:T(128)}, u32[]{:S(2)}) copy-start(f32[32]{0:T(128)} %param.34) | copy-start | bytes 388
  0.1 9.7 %copy-start.20 = (f32[32]{0:T(128)S(1)}, f32[32]{0:T(128)}, u32[]{:S(2)}) copy-start(f32[32]{0:T(128)} %param.33) | copy-start | bytes 388
  0.1 9.7 %copy-start.19 = (f32[32]{0:T(128)S(1)}, f32[32]{0:T(128)}, u32[]{:S(2)}) copy-start(f32[32]{0:T(128)} %param.32) | copy-start | bytes 388
  0.1 9.7 %copy-start.10 = (bf16[2048,32]{0,1:T(8,128)(2,1)S(1)}, bf16[2048,32]{0,1:T(8,128)(2,1)}, u32[]{:S(2)}) copy-start(bf16[2048,32]{0,1:T(8,128)(2,1)} %param.31) | copy-start | bytes 393220
  0.1 9.7 %copy-start.8 = (bf16[2048,256]{1,0:T(8,128)(2,1)S(1)}, bf16[2048,256]{1,0:T(8,128)(2,1)}, u32[]{:S(2)}) copy-start(bf16[2048,256]{1,0:T(8,128)(2,1)} %query_w.1) | copy-start | bytes 3145732
  0.1 9.7 %copy-start.7 = (bf16[2048,256]{1,0:T(8,128)(2,1)S(1)}, bf16[2048,256]{1,0:T(8,128)(2,1)}, u32[]{:S(2)}) copy-start(bf16[2048,256]{1,0:T(8,128)(2,1)} %key_w.1) | copy-start | bytes 3145732
  0.1 9.7 %copy-start.5 = (bf16[2048,512]{1,0:T(8,128)(2,1)S(1)}, bf16[2048,512]{1,0:T(8,128)(2,1)}, u32[]{:S(2)}) copy-start(bf16[2048,512]{1,0:T(8,128)(2,1)} %value_w.1) | copy-start | bytes 6291460
  0.1 9.7 %copy-start.4 = (bf16[2048,512]{1,0:T(8,128)(2,1)S(1)}, bf16[2048,512]{1,0:T(8,128)(2,1)}, u32[]{:S(2)}) copy-start(bf16[2048,512]{1,0:T(8,128)(2,1)} %gate_w.1) | copy-start | bytes 6291460
  0.1 9.7 %copy-start.13 = (f32[2048]{0:T(1024)S(1)}, f32[2048]{0:T(1024)}, u32[]{:S(2)}) copy-start(f32[2048]{0:T(1024)} %param.26) | copy-start | bytes 24580
  0.1 9.7 %copy-start = (f32[48,8,64,128]{3,2,1,0:T(8,128)S(1)}, f32[48,8,64,128]{3,2,1,0:T(8,128)}, u32[]{:S(2)}) copy-start(f32[48,8,64,128]{3,2,1,0:T(8,128)} %param.41) | copy-start | bytes 37748740
  1.1 6.1 %collective-permute-start.2 = (bf16[48,512]{1,0:T(8,128)(2,1)S(1)}, bf16[48,512]{1,0:T(8,128)(2,1)S(1)}, u32[]{:S(2)}, u32[]{:S(2)}) collective-permute-start(bf16[48,512]{1,0:T(8,128)(2,1)S(1)} %entry.1.own_ref), channel_id=1, source_target_pairs={{0,3},{1,2},{2,1},{3,0},{4,7},{5,6},{6,5},{7,4},{8,11},{9,10},{10,... | collective-permute-start | bytes 147464 | tf_op jit(solution)/shard_map/ppermute | solution.py:452
  5.1 4.1 %collective-permute-start.1 = (bf16[48,512]{1,0:T(8,128)(2,1)S(1)}, bf16[48,512]{1,0:T(8,128)(2,1)S(1)}, u32[]{:S(2)}, u32[]{:S(2)}) collective-permute-start(bf16[48,512]{1,0:T(8,128)(2,1)S(1)} %entry.1.own_ref), channel_id=1, source_target_pairs={{0,2},{1,3},{2,0},{3,1},{4,6},{5,7},{6,4},{7,5},{8,10},{9,11},{10,... | collective-permute-start | bytes 147464 | tf_op jit(solution)/shard_map/ppermute | solution.py:452
  5.6 4.1 %collective-permute-start = (bf16[48,512]{1,0:T(8,128)(2,1)S(1)}, bf16[48,512]{1,0:T(8,128)(2,1)S(1)}, u32[]{:S(2)}, u32[]{:S(2)}) collective-permute-start(bf16[48,512]{1,0:T(8,128)(2,1)S(1)} %entry.1.own_ref), channel_id=1, source_target_pairs={{0,1},{1,0},{2,3},{3,2},{4,5},{5,4},{6,7},{7,6},{8,9},{9,8},{10,11... | collective-permute-start | bytes 147464 | tf_op jit(solution)/shard_map/ppermute | solution.py:452
  9.8 6.6 %copy-start.22 = (s32[48,2]{0,1:T(2,128)S(1)}, s32[48,2]{0,1:T(2,128)}, u32[]{:S(2)}) copy-start(s32[48,2]{0,1:T(2,128)} %param.45) | copy-start | bytes 1156
  9.8 6.6 %copy-start.23 = (f32[48,2]{0,1:T(2,128)S(1)}, f32[48,2]{0,1:T(2,128)}, u32[]{:S(2)}) copy-start(f32[48,2]{0,1:T(2,128)} %param.46) | copy-start | bytes 1156
  12.9 4.5 %collective-permute-start.3 = (bf16[48,512]{1,0:T(8,128)(2,1)S(1)}, bf16[48,512]{1,0:T(8,128)(2,1)S(1)}, u32[]{:S(2)}, u32[]{:S(2)}) collective-permute-start(bf16[48,512]{1,0:T(8,128)(2,1)S(1)} %get-tuple-element.15), channel_id=1, source_target_pairs={{0,1},{1,0},{2,3},{3,2},{4,5},{5,4},{6,7},{7,6},{8,9},{9,8},{10,11... | collective-permute-start | bytes 147464 | tf_op jit(solution)/shard_map/ppermute | solution.py:452
  13.4 4.1 %collective-permute-start.4 = (bf16[48,512]{1,0:T(8,128)(2,1)S(1)}, bf16[48,512]{1,0:T(8,128)(2,1)S(1)}, u32[]{:S(2)}, u32[]{:S(2)}) collective-permute-start(bf16[48,512]{1,0:T(8,128)(2,1)S(1)} %get-tuple-element.16), channel_id=1, source_target_pairs={{0,2},{1,3},{2,0},{3,1},{4,6},{5,7},{6,4},{7,5},{8,10},{9,11},{10,... | collective-permute-start | bytes 147464 | tf_op jit(solution)/shard_map/ppermute | solution.py:452
  15.0 5.0 %collective-permute-start.5 = (bf16[48,512]{1,0:T(8,128)(2,1)S(1)}, bf16[48,512]{1,0:T(8,128)(2,1)S(1)}, u32[]{:S(2)}, u32[]{:S(2)}) collective-permute-start(bf16[48,512]{1,0:T(8,128)(2,1)S(1)} %get-tuple-element.17), channel_id=1, source_target_pairs={{0,3},{1,2},{2,1},{3,0},{4,7},{5,6},{6,5},{7,4},{8,11},{9,10},{10,... | collective-permute-start | bytes 147464 | tf_op jit(solution)/shard_map/ppermute | solution.py:452
  16.5 17.0 %copy-start.1 = (bf16[1,2048,1024]{2,1,0:T(8,128)(2,1)S(1)}, bf16[1,2048,1024]{2,1,0:T(8,128)(2,1)}, u32[]{:S(2)}) copy-start(bf16[1,2048,1024]{2,1,0:T(8,128)(2,1)} %param.47) | copy-start | bytes 12582916
  16.5 17.0 %copy-start.2 = (bf16[1,2048,1024]{2,1,0:T(8,128)(2,1)S(1)}, bf16[1,2048,1024]{2,1,0:T(8,128)(2,1)}, u32[]{:S(2)}) copy-start(bf16[1,2048,1024]{2,1,0:T(8,128)(2,1)} %param.48) | copy-start | bytes 12582916
  16.5 17.0 %copy-start.3 = (bf16[1,1024,2048]{2,1,0:T(8,128)(2,1)S(1)}, bf16[1,1024,2048]{2,1,0:T(8,128)(2,1)}, u32[]{:S(2)}) copy-start(bf16[1,1024,2048]{2,1,0:T(8,128)(2,1)} %param.49) | copy-start | bytes 12582916
  16.5 17.0 %copy-start.14 = (f32[2048]{0:T(1024)S(1)}, f32[2048]{0:T(1024)}, u32[]{:S(2)}) copy-start(f32[2048]{0:T(1024)} %param.44) | copy-start | bytes 24580

commit v5 on v4

--- a/solution.py
+++ b/solution.py
@@ -371,8 +371,9 @@
         x_ref[row, column] = line_ref[k, line]
     rows = x_ref[...]
     scale = lax.rsqrt(jnp.mean(rows * rows, axis=-1, keepdims=True) + norm_epsilon)
-    ffn_in = (rows * scale * gain_ref[...]).astype(jnp.bfloat16)
-    hidden = (silu(dot_bf16(ffn_in, gate_w[...])) * dot_bf16(ffn_in, up_w[...])).astype(jnp.bfloat16)
+    raised = (rows * gain_ref[...]).astype(jnp.bfloat16)
+    gate_part = dot_bf16(raised, gate_w[...]) * scale
+    hidden = (silu(gate_part) * (dot_bf16(raised, up_w[...]) * scale)).astype(jnp.bfloat16)
     result = dot_bf16(hidden, down_w[...])
     for row, column, line, k in places:
         line_ref[k, line] = result[row, column]

time: 47.6 us -> 47.5 us (level)
  no operation moved by 1% of the time
where the time goes in v5:
time: 47.5 us; the launch traced here: 47.3 us
  blocking collectives  23.8 us (50%)
  starting transfers between devices  8.2 us (17%)
  Pallas kernels  7.68 us (16%)
  waiting for transfers between devices  7.25 us (15%)
    all_to_all x2, blocking collectives, exchange(): lax.all_to_all(sent, ('tp', 'ep'), split_axis=0, concat_axis=0, tiled=True)  23.8 us
    ppermute x6, starting transfers between devices, shift(): return lax.ppermute(array, 'tp', [(i, i ^ k) for i in range(tp_count)])  8.2 us
    ppermute x6, waiting for transfers between devices, shift(): return lax.ppermute(array, 'tp', [(i, i ^ k) for i in range(tp_count)])  7.25 us
    pallas_call x1, Pallas kernels, local_fast(): pl.pallas_call(mixer_body, out_shape=((pltpu.VMEM((seqs, own_width), f32)...  3.05 us
    pallas_call x1, Pallas kernels, local_fast(): pl.pallas_call(expert_body, out_shape=pltpu.VMEM(moved_shape, bf16), in_s...  2.36 us
  transfers between devices with their start and end apart: 6, of which 6 were waited for; matrix products, arithmetic and copies ran while one was open for 0% of the time, Pallas kernels for 0%

profile of v5, /device:TPU:0, one launch (start us, length us, event | category | flops | bytes accessed | tf_op | source)
XLA Modules:
  0.0 47.3 jit_solution(9153040169735569769)
XLA Ops:
  0.0 0.0 copy-start.6
  0.0 0.0 copy-start.18
  0.0 0.0 copy-start.12
  0.0 0.0 copy-start.17
  0.0 0.0 copy-start.16
  0.0 0.0 copy-start.15
  0.0 0.0 copy-start.21
  0.1 0.0 copy-start.20
  0.1 0.0 copy-start.19
  0.1 0.0 copy-start.10
  0.1 0.0 copy-start.8
  0.1 0.0 copy-start.7
  0.1 0.0 copy-start.5
  0.1 0.0 copy-start.4
  0.1 0.0 copy-start.13
  0.1 0.0 copy-start
  0.1 0.9 %entry.1.own_ref = bf16[48,512]{1,0:T(8,128)(2,1)S(1)} custom-call(bf16[48,512]{1,0:T(8,128)(2,1)} %own_hbm.1), custom_call_target="tpu_custom_call" | custom-call | flops 20000000000 | bytes 33554432 | tf_op jit(solution)/shard_map/entry/pallas_call | solution.py:455
  1.1 4.0 %collective-permute-start.2 = (bf16[48,512]{1,0:T(8,128)(2,1)S(1)}, bf16[48,512]{1,0:T(8,128)(2,1)S(1)}, u32[]{:S(2)}, u32[]{:S(2)}) collective-permute-start(bf16[48,512]{1,0:T(8,128)(2,1)S(1)} %entry.1.own_ref), channel_id=1, source_target_pairs={{0,3},{1,2},{2,1},{3,0},{4,7},{5,6},{6,5},{7,4},{8,11},{9,10},{10,... | collective-permute-start | bytes 147464 | tf_op jit(solution)/shard_map/ppermute | solution.py:453
  5.1 0.5 %collective-permute-start.1 = (bf16[48,512]{1,0:T(8,128)(2,1)S(1)}, bf16[48,512]{1,0:T(8,128)(2,1)S(1)}, u32[]{:S(2)}, u32[]{:S(2)}) collective-permute-start(bf16[48,512]{1,0:T(8,128)(2,1)S(1)} %entry.1.own_ref), channel_id=1, source_target_pairs={{0,2},{1,3},{2,0},{3,1},{4,6},{5,7},{6,4},{7,5},{8,10},{9,11},{10,... | collective-permute-start | bytes 147464 | tf_op jit(solution)/shard_map/ppermute | solution.py:453
  5.6 0.1 collective-permute-start
  5.7 1.4 %collective-permute-done.2.piece_refs_2_ = bf16[48,512]{1,0:T(8,128)(2,1)S(1)} collective-permute-done((bf16[48,512]{1,0:T(8,128)(2,1)S(1)}, bf16[48,512]{1,0:T(8,128)(2,1)S(1)}, u32[]{:S(2)}, u32[]{:S(2)}) %collective-permute-start.2) | collective-permute-done | bytes 49184 | tf_op jit(solution)/shard_map/ppermute | solution.py:453
  7.1 2.0 %collective-permute-done.1.piece_refs_1_ = bf16[48,512]{1,0:T(8,128)(2,1)S(1)} collective-permute-done((bf16[48,512]{1,0:T(8,128)(2,1)S(1)}, bf16[48,512]{1,0:T(8,128)(2,1)S(1)}, u32[]{:S(2)}, u32[]{:S(2)}) %collective-permute-start.1) | collective-permute-done | bytes 49184 | tf_op jit(solution)/shard_map/ppermute | solution.py:453
  9.2 0.5 %collective-permute-done.piece_refs_0_ = bf16[48,512]{1,0:T(8,128)(2,1)S(1)} collective-permute-done((bf16[48,512]{1,0:T(8,128)(2,1)S(1)}, bf16[48,512]{1,0:T(8,128)(2,1)S(1)}, u32[]{:S(2)}, u32[]{:S(2)}) %collective-permute-start) | collective-permute-done | bytes 49184 | tf_op jit(solution)/shard_map/ppermute | solution.py:453
  9.7 0.0 copy-done.6
  9.7 0.0 copy-done.18
  9.7 0.0 copy-done.12
  9.7 0.0 copy-done.11
  9.7 0.0 copy-done.9
  9.7 0.0 copy-done.17
  9.7 0.0 copy-done.16
  9.7 0.0 copy-done.15
  9.7 0.0 copy-done.21
  9.7 0.0 copy-done.20
  9.7 0.0 copy-done.19
  9.8 0.0 copy-done.10
  9.8 0.0 copy-done.8
  9.8 0.0 copy-done.7
  9.8 0.0 copy-done.5
  9.8 0.0 copy-done.4
  9.8 0.0 copy-done.13
  9.8 0.0 copy-done
  9.8 0.0 copy-start.22
  9.8 0.0 copy-start.23
  9.8 3.0 %mixer.1 = (f32[48,512]{1,0:T(8,128)S(1)}, bf16[48,512]{1,0:T(8,128)(2,1)S(1)}, bf16[48,512]{1,0:T(8,128)(2,1)S(1)}, bf16[48,512]{1,0:T(8,128)(2,1)S(1)}) custom-call(bf16[48,512]{1,0:T(8,128)(2,1)S(1)} %entry.1.own_ref, bf16[48,512]{1,0:T(8,128)(2,1)S(1)} %collective-permute-done.piece_refs_0_, bf16[48,512]{1,0:T(8,128)(2,1)S(1)} %collective-permute-done.1.piece_refs_1_, ...), custom_call_target="tpu_custom_call" | custom-call | tf_op jit(solution)/shard_map/mixer/pallas_call | solution.py:479
  12.9 0.5 collective-permute-start.3
  13.4 1.7 %collective-permute-start.4 = (bf16[48,512]{1,0:T(8,128)(2,1)S(1)}, bf16[48,512]{1,0:T(8,128)(2,1)S(1)}, u32[]{:S(2)}, u32[]{:S(2)}) collective-permute-start(bf16[48,512]{1,0:T(8,128)(2,1)S(1)} %get-tuple-element.16), channel_id=1, source_target_pairs={{0,2},{1,3},{2,0},{3,1},{4,6},{5,7},{6,4},{7,5},{8,10},{9,11},{10,... | collective-permute-start | bytes 147464 | tf_op jit(solution)/shard_map/ppermute | solution.py:453
  15.0 1.4 %collective-permute-start.5 = (bf16[48,512]{1,0:T(8,128)(2,1)S(1)}, bf16[48,512]{1,0:T(8,128)(2,1)S(1)}, u32[]{:S(2)}, u32[]{:S(2)}) collective-permute-start(bf16[48,512]{1,0:T(8,128)(2,1)S(1)} %get-tuple-element.17), channel_id=1, source_target_pairs={{0,3},{1,2},{2,1},{3,0},{4,7},{5,6},{6,5},{7,4},{8,11},{9,10},{10,... | collective-permute-start | bytes 147464 | tf_op jit(solution)/shard_map/ppermute | solution.py:453
  16.5 0.0 copy-done.22
  16.5 0.0 copy-done.23
  16.5 0.0 copy-start.3
  16.5 0.0 copy-start.14
  16.5 0.2 route.1
  16.7 0.7 %collective-permute-done.3.part_refs_1_ = bf16[48,512]{1,0:T(8,128)(2,1)S(1)} collective-permute-done((bf16[48,512]{1,0:T(8,128)(2,1)S(1)}, bf16[48,512]{1,0:T(8,128)(2,1)S(1)}, u32[]{:S(2)}, u32[]{:S(2)}) %collective-permute-start.3) | collective-permute-done | bytes 49184 | tf_op jit(solution)/shard_map/ppermute | solution.py:453
  17.4 0.1 collective-permute-done.4.part_refs_2_
  17.5 2.6 %collective-permute-done.5.part_refs_3_ = bf16[48,512]{1,0:T(8,128)(2,1)S(1)} collective-permute-done((bf16[48,512]{1,0:T(8,128)(2,1)S(1)}, bf16[48,512]{1,0:T(8,128)(2,1)S(1)}, u32[]{:S(2)}, u32[]{:S(2)}) %collective-permute-start.5) | collective-permute-done | bytes 49184 | tf_op jit(solution)/shard_map/ppermute | solution.py:453
  20.0 0.2 pack.1
  20.3 13.2 %all_to_all.10.arrived_ref = bf16[32,4,640]{2,1,0:T(4,128)(2,1)S(1)} all-to-all(bf16[32,4,640]{2,1,0:T(4,128)(2,1)S(1)} %get-tuple-element.19), channel_id=1, replica_groups=mesh['ep'=8,'tp'=4] {'tp','ep'}, dimensions={0} | all-to-all | bytes 327680 | tf_op jit(solution)/shard_map/all_to_all | solution.py:527
  33.5 0.0 copy-done.1
  33.5 0.0 copy-done.2
  33.5 0.0 copy-done.3
  33.5 0.0 copy-done.14
  33.5 2.4 %expert.1 = bf16[32,4,640]{2,1,0:T(4,128)(2,1)S(1)} custom-call(bf16[32,4,640]{2,1,0:T(4,128)(2,1)S(1)} %all_to_all.10.arrived_ref, f32[1,2048]{1,0:T(1,128)S(1)} %bitcast.25, bf16[2048,1024]{1,0:T(8,128)(2,1)S(1)} %bitcast.17, bf16[2048,1024]{1,0:T(8,128)(2,1)S(1)} %bitcast.18, bf16[1024,2048]{1,0:T(8,128)(2,1)S(1)} %bitcast.19), custom_call_target="tpu_custom_call" | custom-call | tf_op jit(solution)/shard_map/expert/pallas_call | solution.py:529
  35.9 10.5 %all_to_all.11.returned_ref = bf16[32,4,640]{2,1,0:T(4,128)(2,1)S(1)} all-to-all(bf16[32,4,640]{2,1,0:T(4,128)(2,1)S(1)} %expert.1), channel_id=1, replica_groups=mesh['ep'=8,'tp'=4] {'tp','ep'}, dimensions={0} | all-to-all | bytes 327680 | tf_op jit(solution)/shard_map/all_to_all | solution.py:527
  46.4 0.9 %combine.1 = bf16[48,512]{1,0:T(8,128)(2,1)} custom-call(bf16[32,4,640]{2,1,0:T(4,128)(2,1)S(1)} %all_to_all.11.returned_ref, bf16[48,512]{1,0:T(8,128)(2,1)S(1)} %get-tuple-element.20.residual_ref, bf16[48,160]{1,0:T(8,128)(2,1)S(1)} %get-tuple-element.21.high_ref, bf16[48,160]{1,0:T(8,128)(2,1)S(1)} %get-tuple-element.22.low_ref), custom_call_target="tpu_custom_call" | custom-call | tf_op jit(solution)/shard_map/combine/pallas_call | solution.py:544
  (4 shorter events, 0.0 us)
Async XLA Ops:
  0.0 9.7 %copy-start.6 = (bf16[512,2048]{1,0:T(8,128)(2,1)S(1)}, bf16[512,2048]{1,0:T(8,128)(2,1)}, u32[]{:S(2)}) copy-start(bf16[512,2048]{1,0:T(8,128)(2,1)} %out_w.1) | copy-start | bytes 6291460
  0.0 9.7 %copy-start.18 = (f32[512]{0:T(512)S(1)}, f32[512]{0:T(512)}, u32[]{:S(2)}) copy-start(f32[512]{0:T(512)} %param.42) | copy-start | bytes 6148
  0.0 9.7 %copy-start.12 = (bf16[48,3,256]{2,0,1:T(8,128)(2,1)S(1)}, bf16[48,3,256]{2,0,1:T(8,128)(2,1)}, u32[]{:S(2)}) copy-start(bf16[48,3,256]{2,0,1:T(8,128)(2,1)} %param.40) | copy-start | bytes 221188
  0.0 9.7 %copy-start.11 = (bf16[48,3,256]{2,0,1:T(8,128)(2,1)S(1)}, bf16[48,3,256]{2,0,1:T(8,128)(2,1)}, u32[]{:S(2)}) copy-start(bf16[48,3,256]{2,0,1:T(8,128)(2,1)} %param.39) | copy-start | bytes 221188
  0.0 9.7 %copy-start.9 = (bf16[48,3,512]{2,0,1:T(8,128)(2,1)S(1)}, bf16[48,3,512]{2,0,1:T(8,128)(2,1)}, u32[]{:S(2)}) copy-start(bf16[48,3,512]{2,0,1:T(8,128)(2,1)} %param.38) | copy-start | bytes 442372
  0.0 9.7 %copy-start.17 = (bf16[4,256]{1,0:T(4,128)(2,1)S(1)}, bf16[4,256]{1,0:T(4,128)(2,1)}, u32[]{:S(2)}) copy-start(bf16[4,256]{1,0:T(4,128)(2,1)} %tap_c_ref.1) | copy-start | bytes 6148
  0.0 9.7 %copy-start.16 = (bf16[4,256]{1,0:T(4,128)(2,1)S(1)}, bf16[4,256]{1,0:T(4,128)(2,1)}, u32[]{:S(2)}) copy-start(bf16[4,256]{1,0:T(4,128)(2,1)} %tap_b_ref.1) | copy-start | bytes 6148
  0.0 9.7 %copy-start.15 = (bf16[4,512]{1,0:T(4,128)(2,1)S(1)}, bf16[4,512]{1,0:T(4,128)(2,1)}, u32[]{:S(2)}) copy-start(bf16[4,512]{1,0:T(4,128)(2,1)} %tap_x_ref.1) | copy-start | bytes 12292
  0.0 9.7 %copy-start.21 = (f32[32]{0:T(128)S(1)}, f32[32]{0:T(128)}, u32[]{:S(2)}) copy-start(f32[32]{0:T(128)} %param.34) | copy-start | bytes 388
  0.1 9.7 %copy-start.20 = (f32[32]{0:T(128)S(1)}, f32[32]{0:T(128)}, u32[]{:S(2)}) copy-start(f32[32]{0:T(128)} %param.33) | copy-start | bytes 388
  0.1 9.7 %copy-start.19 = (f32[32]{0:T(128)S(1)}, f32[32]{0:T(128)}, u32[]{:S(2)}) copy-start(f32[32]{0:T(128)} %param.32) | copy-start | bytes 388
  0.1 9.7 %copy-start.10 = (bf16[2048,32]{0,1:T(8,128)(2,1)S(1)}, bf16[2048,32]{0,1:T(8,128)(2,1)}, u32[]{:S(2)}) copy-start(bf16[2048,32]{0,1:T(8,128)(2,1)} %param.31) | copy-start | bytes 393220
  0.1 9.7 %copy-start.8 = (bf16[2048,256]{1,0:T(8,128)(2,1)S(1)}, bf16[2048,256]{1,0:T(8,128)(2,1)}, u32[]{:S(2)}) copy-start(bf16[2048,256]{1,0:T(8,128)(2,1)} %query_w.1) | copy-start | bytes 3145732
  0.1 9.7 %copy-start.7 = (bf16[2048,256]{1,0:T(8,128)(2,1)S(1)}, bf16[2048,256]{1,0:T(8,128)(2,1)}, u32[]{:S(2)}) copy-start(bf16[2048,256]{1,0:T(8,128)(2,1)} %key_w.1) | copy-start | bytes 3145732
  0.1 9.7 %copy-start.5 = (bf16[2048,512]{1,0:T(8,128)(2,1)S(1)}, bf16[2048,512]{1,0:T(8,128)(2,1)}, u32[]{:S(2)}) copy-start(bf16[2048,512]{1,0:T(8,128)(2,1)} %value_w.1) | copy-start | bytes 6291460
  0.1 9.7 %copy-start.4 = (bf16[2048,512]{1,0:T(8,128)(2,1)S(1)}, bf16[2048,512]{1,0:T(8,128)(2,1)}, u32[]{:S(2)}) copy-start(bf16[2048,512]{1,0:T(8,128)(2,1)} %gate_w.1) | copy-start | bytes 6291460
  0.1 9.7 %copy-start.13 = (f32[2048]{0:T(1024)S(1)}, f32[2048]{0:T(1024)}, u32[]{:S(2)}) copy-start(f32[2048]{0:T(1024)} %param.26) | copy-start | bytes 24580
  0.1 9.7 %copy-start = (f32[48,8,64,128]{3,2,1,0:T(8,128)S(1)}, f32[48,8,64,128]{3,2,1,0:T(8,128)}, u32[]{:S(2)}) copy-start(f32[48,8,64,128]{3,2,1,0:T(8,128)} %param.41) | copy-start | bytes 37748740
  1.1 6.1 %collective-permute-start.2 = (bf16[48,512]{1,0:T(8,128)(2,1)S(1)}, bf16[48,512]{1,0:T(8,128)(2,1)S(1)}, u32[]{:S(2)}, u32[]{:S(2)}) collective-permute-start(bf16[48,512]{1,0:T(8,128)(2,1)S(1)} %entry.1.own_ref), channel_id=1, source_target_pairs={{0,3},{1,2},{2,1},{3,0},{4,7},{5,6},{6,5},{7,4},{8,11},{9,10},{10,... | collective-permute-start | bytes 147464 | tf_op jit(solution)/shard_map/ppermute | solution.py:453
  5.1 4.1 %collective-permute-start.1 = (bf16[48,512]{1,0:T(8,128)(2,1)S(1)}, bf16[48,512]{1,0:T(8,128)(2,1)S(1)}, u32[]{:S(2)}, u32[]{:S(2)}) collective-permute-start(bf16[48,512]{1,0:T(8,128)(2,1)S(1)} %entry.1.own_ref), channel_id=1, source_target_pairs={{0,2},{1,3},{2,0},{3,1},{4,6},{5,7},{6,4},{7,5},{8,10},{9,11},{10,... | collective-permute-start | bytes 147464 | tf_op jit(solution)/shard_map/ppermute | solution.py:453
  5.6 4.1 %collective-permute-start = (bf16[48,512]{1,0:T(8,128)(2,1)S(1)}, bf16[48,512]{1,0:T(8,128)(2,1)S(1)}, u32[]{:S(2)}, u32[]{:S(2)}) collective-permute-start(bf16[48,512]{1,0:T(8,128)(2,1)S(1)} %entry.1.own_ref), channel_id=1, source_target_pairs={{0,1},{1,0},{2,3},{3,2},{4,5},{5,4},{6,7},{7,6},{8,9},{9,8},{10,11... | collective-permute-start | bytes 147464 | tf_op jit(solution)/shard_map/ppermute | solution.py:453
  9.8 6.6 %copy-start.22 = (s32[48,2]{0,1:T(2,128)S(1)}, s32[48,2]{0,1:T(2,128)}, u32[]{:S(2)}) copy-start(s32[48,2]{0,1:T(2,128)} %param.45) | copy-start | bytes 1156
  9.8 6.6 %copy-start.23 = (f32[48,2]{0,1:T(2,128)S(1)}, f32[48,2]{0,1:T(2,128)}, u32[]{:S(2)}) copy-start(f32[48,2]{0,1:T(2,128)} %param.46) | copy-start | bytes 1156
  12.9 4.5 %collective-permute-start.3 = (bf16[48,512]{1,0:T(8,128)(2,1)S(1)}, bf16[48,512]{1,0:T(8,128)(2,1)S(1)}, u32[]{:S(2)}, u32[]{:S(2)}) collective-permute-start(bf16[48,512]{1,0:T(8,128)(2,1)S(1)} %get-tuple-element.15), channel_id=1, source_target_pairs={{0,1},{1,0},{2,3},{3,2},{4,5},{5,4},{6,7},{7,6},{8,9},{9,8},{10,11... | collective-permute-start | bytes 147464 | tf_op jit(solution)/shard_map/ppermute | solution.py:453
  13.4 4.1 %collective-permute-start.4 = (bf16[48,512]{1,0:T(8,128)(2,1)S(1)}, bf16[48,512]{1,0:T(8,128)(2,1)S(1)}, u32[]{:S(2)}, u32[]{:S(2)}) collective-permute-start(bf16[48,512]{1,0:T(8,128)(2,1)S(1)} %get-tuple-element.16), channel_id=1, source_target_pairs={{0,2},{1,3},{2,0},{3,1},{4,6},{5,7},{6,4},{7,5},{8,10},{9,11},{10,... | collective-permute-start | bytes 147464 | tf_op jit(solution)/shard_map/ppermute | solution.py:453
  15.0 5.0 %collective-permute-start.5 = (bf16[48,512]{1,0:T(8,128)(2,1)S(1)}, bf16[48,512]{1,0:T(8,128)(2,1)S(1)}, u32[]{:S(2)}, u32[]{:S(2)}) collective-permute-start(bf16[48,512]{1,0:T(8,128)(2,1)S(1)} %get-tuple-element.17), channel_id=1, source_target_pairs={{0,3},{1,2},{2,1},{3,0},{4,7},{5,6},{6,5},{7,4},{8,11},{9,10},{10,... | collective-permute-start | bytes 147464 | tf_op jit(solution)/shard_map/ppermute | solution.py:453
  16.5 17.0 %copy-start.1 = (bf16[1,2048,1024]{2,1,0:T(8,128)(2,1)S(1)}, bf16[1,2048,1024]{2,1,0:T(8,128)(2,1)}, u32[]{:S(2)}) copy-start(bf16[1,2048,1024]{2,1,0:T(8,128)(2,1)} %param.47) | copy-start | bytes 12582916
  16.5 17.0 %copy-start.2 = (bf16[1,2048,1024]{2,1,0:T(8,128)(2,1)S(1)}, bf16[1,2048,1024]{2,1,0:T(8,128)(2,1)}, u32[]{:S(2)}) copy-start(bf16[1,2048,1024]{2,1,0:T(8,128)(2,1)} %param.48) | copy-start | bytes 12582916
  16.5 17.0 %copy-start.3 = (bf16[1,1024,2048]{2,1,0:T(8,128)(2,1)S(1)}, bf16[1,1024,2048]{2,1,0:T(8,128)(2,1)}, u32[]{:S(2)}) copy-start(bf16[1,1024,2048]{2,1,0:T(8,128)(2,1)} %param.49) | copy-start | bytes 12582916
  16.5 17.0 %copy-start.14 = (f32[2048]{0:T(1024)S(1)}, f32[2048]{0:T(1024)}, u32[]{:S(2)}) copy-start(f32[2048]{0:T(1024)} %param.44) | copy-start | bytes 24580
